TPU v7x, 128 devices: a whole 4x4x4 slice. The times are simulated.
128 devices in a mesh: sp: 32 (over z, y, core), tp: 4 (over x).
Axes of the slice: x: 4, y: 4, z: 4, core: 2. Of those that a mesh axis runs over, the one named last changes fastest.
Arguments:
- tokens: bfloat16 [4096, 1024], P('sp', 'tp'), may hold values from -6 to 6
- norm_gain: float32 [1024], replicated, may hold values from 0.1 to 1.9
- attn_query: bfloat16 [1024, 512], P('sp', 'tp'), may hold values from -0.1875 to 0.1875
- attn_key: bfloat16 [1024, 256], P('sp', 'tp'), may hold values from -0.1875 to 0.1875
- attn_value: bfloat16 [1024, 256], P('sp', 'tp'), may hold values from -0.1875 to 0.1875
- sink_logit: float32 [8], P('tp'), may hold values from 2 to 7
- delta_query: bfloat16 [1024, 512], P('sp', 'tp'), may hold values from -0.1875 to 0.1875
- delta_key: bfloat16 [1024, 512], P('sp', 'tp'), may hold values from -0.1875 to 0.1875
- delta_value: bfloat16 [1024, 512], P('sp', 'tp'), may hold values from -0.1875 to 0.1875
- delta_gate: bfloat16 [1024, 512], P('sp', 'tp'), may hold values from -0.1875 to 0.1875
- beta_weight: bfloat16 [1024, 8, 2], P('sp', 'tp'), may hold values from -0.1875 to 0.1875
- decay_weight: bfloat16 [1024, 8, 2], P('sp', 'tp'), may hold values from -0.1875 to 0.1875
- beta_shift: float32 [2, 8], P(None, 'tp'), may hold values from -5 to -2
- decay_log: float32 [2, 8], P(None, 'tp'), may hold values from -2.5 to 1
- out_gain: float32 [64], replicated, may hold values from 0.1 to 1.9
- attn_out: bfloat16 [512, 1024], P('tp', 'sp'), may hold values from -1.5 to 1.5
- delta_out: bfloat16 [512, 1024], P('tp', 'sp'), may hold values from -0.25 to 0.25
Outputs:
- mixed: bfloat16 [4096, 1024], P(('sp', 'tp'))
All inputs are finite; a program needn't handle non-finite values.
Results may differ from a plain program's by a relative error of at most 0.0045.
Values may be sent and summed in bfloat16 or wider, within the bound.
A program may use at most 64 MiB of HBM per device.

v0:
```python
import jax
import jax.numpy as jnp
from jax import lax
from jax.sharding import PartitionSpec as P

HEAD_DIM = 64
WINDOW = 64
BLOCK_LEN = 32


norm_eps = 1e-06
highest = lax.Precision.HIGHEST


def prefix(part, axis, combine, identity, reverse):
    count = lax.axis_size(axis)
    place = lax.axis_index(axis)
    ahead = count - 1 - place if reverse else place
    gathered = jax.tree.map(lambda a: lax.all_gather(a, axis), part)
    state = jax.tree.map(lambda a, e: jnp.zeros_like(a) + jnp.asarray(e, a.dtype), part, identity)

    def one(turn, state):
        source = count - 1 - turn if reverse else turn
        return combine(
            state, jax.tree.map(lambda a: lax.dynamic_index_in_dim(a, source, 0, False), gathered)
        )

    return lax.fori_loop(0, ahead, one, state)


def extended(cells, sides, width, closed):
    for axis, dim in sides:
        count = lax.axis_size(axis)
        ends = count if closed else count - 1
        head = lax.slice_in_dim(cells, 0, width, axis=dim)
        tail = lax.slice_in_dim(cells, cells.shape[dim] - width, cells.shape[dim], axis=dim)
        cells = jnp.concatenate(
            [
                lax.ppermute(tail, axis, [(i, (i + 1) % count) for i in range(ends)]),
                cells,
                lax.ppermute(head, axis, [((i + 1) % count, i) for i in range(ends)]),
            ],
            axis=dim,
        )
    return cells


def rounded(values):
    return lax.optimization_barrier(values.astype(jnp.bfloat16))


def unit_rows(values):
    return values * lax.rsqrt(jnp.sum(values * values, axis=-1, keepdims=True) + norm_eps)


def block_pass(queries, key_rows, value_rows, log_decay, strength, initial):
    row_count, head_count = (queries.shape[0], queries.shape[1])
    value_width = value_rows.shape[2]
    block_count = row_count // BLOCK_LEN

    def blocks(values):
        return values.reshape(block_count, BLOCK_LEN, head_count, -1).transpose(0, 2, 1, 3)

    q_blocks, k_blocks, v_blocks = (blocks(queries), blocks(key_rows), blocks(value_rows))
    cumulative = jnp.cumsum(
        log_decay.reshape(block_count, BLOCK_LEN, head_count).transpose(0, 2, 1), axis=-1
    )
    beta_blocks = strength.reshape(block_count, BLOCK_LEN, head_count).transpose(0, 2, 1)
    lower_mask = jnp.tril(jnp.ones((BLOCK_LEN, BLOCK_LEN), jnp.bool_))
    strict = jnp.tril(jnp.ones((BLOCK_LEN, BLOCK_LEN), jnp.bool_), -1)
    decay_mat = jnp.exp(
        jnp.where(lower_mask, cumulative[..., :, None] - cumulative[..., None, :], -jnp.inf)
    )
    k_beta = k_blocks * beta_blocks[..., None]
    lower_mat = jnp.where(
        strict, jnp.einsum("nhcd,nhmd->nhcm", k_beta, k_blocks, precision=highest) * decay_mat, 0.0
    )
    system = lower_mat + jnp.eye(BLOCK_LEN, dtype=jnp.float32)
    right_side = jnp.concatenate(
        [v_blocks * beta_blocks[..., None], k_beta * jnp.exp(cumulative)[..., None]], axis=-1
    )
    solved = lax.linalg.triangular_solve(
        system, right_side, left_side=True, lower=True, unit_diagonal=True
    )
    pad_width = initial.shape[2] - value_width
    pseudo = jnp.pad(solved[..., :value_width], ((0, 0), (0, 0), (0, 0), (0, pad_width)))
    key_decay = solved[..., value_width:]
    scores = jnp.einsum("nhcd,nhmd->nhcm", q_blocks, k_blocks, precision=highest) * decay_mat
    last_decay = cumulative[..., -1]
    q_inner = q_blocks * jnp.exp(cumulative)[..., None]
    k_update = k_blocks * jnp.exp(last_decay[..., None] - cumulative)[..., None]

    def advance(carry_state, inputs):
        q_row, k_row, u_row, w_row, s_row, g_row = inputs
        fresh_values = u_row - jnp.einsum("hcd,hde->hce", w_row, carry_state, precision=highest)
        output = jnp.einsum("hcd,hde->hce", q_row, carry_state, precision=highest) + jnp.einsum(
            "hcm,hme->hce", s_row, fresh_values, precision=highest
        )
        carry_state = carry_state * jnp.exp(g_row)[:, None, None] + jnp.einsum(
            "hcd,hce->hde", k_row, fresh_values, precision=highest
        )
        return (carry_state, output)

    final_state, outputs = lax.scan(
        advance, initial, (q_inner, k_update, pseudo, key_decay, scores, last_decay)
    )
    return (final_state, outputs.transpose(0, 2, 1, 3).reshape(row_count, head_count, -1))


def compose(earlier_map, later_map):
    return (
        jnp.einsum("hij,hjk->hik", later_map[0], earlier_map[0], precision=highest),
        jnp.einsum("hij,hjk->hik", later_map[0], earlier_map[1], precision=highest) + later_map[1],
    )


def delta_chains(fore_args, back_args):
    head_count, key_width = (fore_args[0].shape[1], fore_args[0].shape[2])
    value_width = fore_args[2].shape[2]
    eye_stack = jnp.broadcast_to(
        jnp.eye(key_width, dtype=jnp.float32), (head_count, key_width, key_width)
    )
    start_state = jnp.concatenate(
        [jnp.zeros((head_count, key_width, value_width), jnp.float32), eye_stack], axis=-1
    )
    fore_final, fore_outs = block_pass(
        fore_args[0], fore_args[1], fore_args[2], fore_args[3], fore_args[4], start_state
    )
    back_final, back_outs = block_pass(
        back_args[0], back_args[1], back_args[2], back_args[3], back_args[4], start_state
    )
    identity = (eye_stack, jnp.zeros((head_count, key_width, value_width), jnp.float32))
    fore_in = prefix(
        (fore_final[..., value_width:], fore_final[..., :value_width]),
        "sp",
        compose,
        identity,
        False,
    )[1]
    back_in = prefix(
        (back_final[..., value_width:], back_final[..., :value_width]),
        "sp",
        compose,
        identity,
        True,
    )[1]
    return (fore_in, back_in, fore_outs, back_outs)


def delta_finish(chains, fore_args, back_args, gate_rows, out_gain):
    fore_in, back_in, fore_outs, back_outs = chains
    fore_rows = block_pass(
        fore_args[0], fore_args[1], fore_args[2], fore_args[3], fore_args[4], fore_in
    )[1]
    back_rows = block_pass(
        back_args[0], back_args[1], back_args[2], back_args[3], back_args[4], back_in
    )[1]
    both_ways = fore_rows + jnp.flip(back_rows, 0)
    normed_out = (
        both_ways
        * lax.rsqrt(jnp.mean(both_ways * both_ways, axis=-1, keepdims=True) + norm_eps)
        * out_gain
    )
    gated = (normed_out * jax.nn.silu(gate_rows)).astype(jnp.bfloat16)
    return gated.reshape(gated.shape[0], -1)


def window_attention(att_q, att_k, att_v, sink_logit):
    row_count = att_q.shape[0]
    kv_count = att_k.shape[1] // HEAD_DIM
    group_size = att_q.shape[1] // HEAD_DIM // kv_count
    paired = jnp.concatenate([att_k, att_v], axis=1)
    padded = extended(paired, (("sp", 0),), WINDOW, False)
    key_rows = padded[:, : kv_count * HEAD_DIM].reshape(-1, kv_count, HEAD_DIM)
    value_rows = padded[:, kv_count * HEAD_DIM :].reshape(-1, kv_count, HEAD_DIM)
    total_rows = row_count * lax.axis_size("sp")
    offset = lax.axis_index("sp") * row_count
    q_pos = offset + jnp.arange(row_count, dtype=jnp.int32)
    k_pos = offset - WINDOW + jnp.arange(row_count + 2 * WINDOW, dtype=jnp.int32)
    allowed = (
        (jnp.abs(q_pos[:, None] - k_pos[None, :]) <= WINDOW)
        & (k_pos[None, :] >= 0)
        & (k_pos[None, :] < total_rows)
    )
    queries = att_q.reshape(row_count, kv_count, group_size, HEAD_DIM)
    scores = jnp.einsum(
        "tkgd,jkd->kgtj", queries, key_rows, preferred_element_type=jnp.float32
    ) * HEAD_DIM ** (-0.5)
    scores = jnp.where(allowed, scores, -jnp.inf)
    sink_row = sink_logit.reshape(kv_count, group_size, 1, 1)
    row_max = jnp.maximum(jnp.max(scores, axis=-1, keepdims=True), sink_row)
    weights = jnp.exp(scores - row_max)
    weights = weights / (jnp.sum(weights, axis=-1, keepdims=True) + jnp.exp(sink_row - row_max))
    heads_out = jnp.einsum(
        "kgtj,jkd->tkgd",
        weights.astype(jnp.bfloat16),
        value_rows,
        preferred_element_type=jnp.float32,
    )
    return heads_out.reshape(row_count, -1).astype(jnp.bfloat16)


def per_device(
    tokens,
    norm_gain,
    attn_query,
    attn_key,
    attn_value,
    sink_logit,
    delta_query,
    delta_key,
    delta_value,
    delta_gate,
    beta_weight,
    decay_weight,
    beta_shift,
    decay_log,
    out_gain,
    attn_out,
    delta_out,
):
    row_count = tokens.shape[0]
    whole_rows = lax.all_gather(tokens, "tp", axis=1, tiled=True)
    wide_rows = whole_rows.astype(jnp.float32)
    inverse = lax.rsqrt(jnp.mean(wide_rows * wide_rows, axis=-1, keepdims=True) + norm_eps)
    normed = (wide_rows * inverse * norm_gain).astype(jnp.bfloat16)
    beta_flat = beta_weight.reshape(beta_weight.shape[0], -1)
    decay_flat = decay_weight.reshape(decay_weight.shape[0], -1)

    def add_rows(totals, pieces):
        columns = lax.slice_in_dim(normed, 0, pieces[0].shape[0], axis=1)
        return tuple(
            (
                total_sum + jnp.dot(columns, piece_rows, preferred_element_type=jnp.float32)
                for total_sum, piece_rows in zip(totals, pieces)
            )
        )

    empty_sums = tuple(
        (
            jnp.zeros((row_count, weight_part.shape[1]), jnp.float32)
            for weight_part in (
                attn_query,
                attn_key,
                attn_value,
                delta_query,
                delta_key,
                delta_value,
                delta_gate,
                beta_flat,
                decay_flat,
            )
        )
    )
    p_aq, p_ak, p_av, p_dq, p_dk, p_dv, p_dz, p_beta, p_decay = add_rows(
        empty_sums,
        (
            lax.all_gather(attn_query, "sp", axis=0, tiled=True),
            lax.all_gather(attn_key, "sp", axis=0, tiled=True),
            lax.all_gather(attn_value, "sp", axis=0, tiled=True),
            lax.all_gather(delta_query, "sp", axis=0, tiled=True),
            lax.all_gather(delta_key, "sp", axis=0, tiled=True),
            lax.all_gather(delta_value, "sp", axis=0, tiled=True),
            lax.all_gather(delta_gate, "sp", axis=0, tiled=True),
            lax.all_gather(beta_flat, "sp", axis=0, tiled=True),
            lax.all_gather(decay_flat, "sp", axis=0, tiled=True),
        ),
    )
    att_q = p_aq.astype(jnp.bfloat16)
    att_k = p_ak.astype(jnp.bfloat16)
    att_v = p_av.astype(jnp.bfloat16)
    head_count = delta_query.shape[1] // HEAD_DIM
    sequence_rows = row_count * lax.axis_size("sp")

    def activate(projection):
        return jax.nn.silu(rounded(projection).astype(jnp.float32)).reshape(
            row_count, head_count, HEAD_DIM
        )

    d_query = unit_rows(activate(p_dq)) * HEAD_DIM ** (-0.5)
    d_key = unit_rows(activate(p_dk))
    d_value = activate(p_dv)
    gate_rows = rounded(p_dz).astype(jnp.float32).reshape(row_count, head_count, HEAD_DIM)
    strength = jax.nn.sigmoid(p_beta.reshape(row_count, head_count, 2) + beta_shift.T)
    log_decay = (
        -jnp.exp(decay_log.T)
        * jax.nn.softplus(p_decay.reshape(row_count, head_count, 2))
        / sequence_rows
    )
    fore_args = (d_query, d_key, d_value, log_decay[:, :, 0], strength[:, :, 0])
    back_args = (
        jnp.flip(d_query, 0),
        jnp.flip(d_key, 0),
        jnp.flip(d_value, 0),
        jnp.flip(log_decay[:, :, 1], 0),
        jnp.flip(strength[:, :, 1], 0),
    )
    y_attn = window_attention(att_q, att_k, att_v, sink_logit)
    chains = delta_chains(fore_args, back_args)
    y_delta = delta_finish(chains, fore_args, back_args, gate_rows, out_gain)
    joined = jnp.concatenate([y_attn, y_delta], axis=1)
    stacked = jnp.concatenate([attn_out, delta_out], axis=0)
    full_weight = lax.all_gather(stacked, "sp", axis=1, tiled=True)

    def term_rows():
        return jnp.dot(
            lax.slice_in_dim(
                joined, 0, lax.axis_size("tp") * (row_count // lax.axis_size("tp")), axis=0
            ),
            full_weight,
            preferred_element_type=jnp.float32,
        )

    summed = lax.psum_scatter(term_rows(), "tp", scatter_dimension=0, tiled=True)
    return summed.astype(jnp.bfloat16)


def solution(mesh):
    return jax.shard_map(
        per_device,
        mesh=mesh,
        in_specs=(
            P("sp", "tp"),
            P(),
            P("sp", "tp"),
            P("sp", "tp"),
            P("sp", "tp"),
            P("tp"),
            P("sp", "tp"),
            P("sp", "tp"),
            P("sp", "tp"),
            P("sp", "tp"),
            P("sp", "tp", None),
            P("sp", "tp", None),
            P(None, "tp"),
            P(None, "tp"),
            P(),
            P("tp", "sp"),
            P("tp", "sp"),
        ),
        out_specs=P(("sp", "tp"), None),
        check_vma=False,
    )
```

profile of v0, /device:TPU:1, one launch (start us, length us, event | category | flops | bytes accessed | tf_op | source)
XLA Modules:
  0.0 434.5 jit_solution(11189347355040340770)
XLA Ops:
  6.5 11.3 %all_gather.57 = bf16[128,1024]{1,0:T(8,128)(2,1)S(1)} all-gather(bf16[128,256]{1,0:T(8,128)(2,1)} %param.31), channel_id=1, replica_groups=mesh['sp'=32,'tp'=4] {'tp'}, dimensions={1}, use_global_device_ids=true | all-gather | bytes 327680 | tf_op jit(solution)/shard_map/all_gather | solution.py:223
  18.0 29.1 %all_gather.62 = bf16[1024,128]{1,0:T(8,128)(2,1)S(1)} all-gather(bf16[32,128]{1,0:T(8,128)(2,1)} %param.38), channel_id=1, replica_groups=mesh['sp'=32,'tp'=4] {'sp'}, dimensions={0}, use_global_device_ids=true | all-gather | bytes 270336 | tf_op jit(solution)/shard_map/all_gather | solution.py:262
  48.4 24.1 %all_gather.69 = bf16[1024,128]{1,0:T(8,128)(2,1)S(1)} all-gather(bf16[32,128]{1,0:T(8,128)(2,1)} %param.37), channel_id=1, replica_groups=mesh['sp'=32,'tp'=4] {'sp'}, dimensions={0}, use_global_device_ids=true | all-gather | bytes 270336 | tf_op jit(solution)/shard_map/all_gather | solution.py:261
  73.4 22.4 %all_gather.64 = bf16[1024,128]{1,0:T(8,128)(2,1)S(1)} all-gather(bf16[32,128]{1,0:T(8,128)(2,1)S(1)} %copy-done), channel_id=1, replica_groups=mesh['sp'=32,'tp'=4] {'sp'}, dimensions={0}, use_global_device_ids=true | all-gather | bytes 270336 | tf_op jit(solution)/shard_map/all_gather | solution.py:263
  96.4 23.7 %all-gather.4 = bf16[32,32,4]{1,2,0:T(4,128)(2,1)S(1)} all-gather(bf16[1,32,4]{1,2,0:T(4,128)(2,1)S(1)} %bitcast.327), channel_id=1, replica_groups=mesh['sp'=32,'tp'=4] {'sp'}, dimensions={0}, use_global_device_ids=true | all-gather | bytes 8448 | tf_op jit(solution)/shard_map/all_gather | solution.py:266
  122.3 22.0 %all-gather.5 = bf16[32,32,4]{1,2,0:T(4,128)(2,1)S(1)} all-gather(bf16[1,32,4]{1,2,0:T(4,128)(2,1)S(1)} %bitcast.328), channel_id=1, replica_groups=mesh['sp'=32,'tp'=4] {'sp'}, dimensions={0}, use_global_device_ids=true | all-gather | bytes 8448 | tf_op jit(solution)/shard_map/all_gather | solution.py:265
  147.2 19.7 %custom-call.4 = f32[4,2,1,32,32]{3,4,2,1,0:T(8,128)S(1)} custom-call(f32[4,2,1,32,32]{4,3,2,1,0:T(8,128)S(1)} %fusion.67), custom_call_target="InvertDiagBlocksLowerTriangular" | custom-call | tf_op jit(solution)/shard_map/triangular_solve/custom-call.1 | solution.py:82
  167.3 19.7 %custom-call.5 = f32[4,2,1,32,32]{3,4,2,1,0:T(8,128)S(1)} custom-call(f32[4,2,1,32,32]{4,3,2,1,0:T(8,128)S(1)} %fusion.62), custom_call_target="InvertDiagBlocksLowerTriangular" | custom-call | tf_op jit(solution)/shard_map/triangular_solve/custom-call.1 | solution.py:82
  188.6 2.1 while.73
  192.4 2.1 while.70
  195.4 24.3 %all_gather.59 = bf16[1024,64]{1,0:T(8,128)(2,1)S(1)} all-gather(bf16[32,64]{1,0:T(8,128)(2,1)S(1)} %copy-done.1), channel_id=1, replica_groups=mesh['sp'=32,'tp'=4] {'sp'}, dimensions={0}, use_global_device_ids=true | all-gather | bytes 135168 | tf_op jit(solution)/shard_map/all_gather | solution.py:260
  219.7 22.4 %all_gather.58 = bf16[1024,64]{1,0:T(8,128)(2,1)S(1)} all-gather(bf16[32,64]{1,0:T(8,128)(2,1)S(1)} %copy-done.2), channel_id=1, replica_groups=mesh['sp'=32,'tp'=4] {'sp'}, dimensions={0}, use_global_device_ids=true | all-gather | bytes 135168 | tf_op jit(solution)/shard_map/all_gather | solution.py:259
  242.7 2.9 collective-permute-start
  245.7 1.9 collective-permute-start.1
  248.5 27.0 %all_gather.60 = bf16[1024,128]{1,0:T(8,128)(2,1)S(1)} all-gather(bf16[32,128]{1,0:T(8,128)(2,1)S(1)} %copy-done.3), channel_id=1, replica_groups=mesh['sp'=32,'tp'=4] {'sp'}, dimensions={0}, use_global_device_ids=true | all-gather | bytes 270336 | tf_op jit(solution)/shard_map/all_gather | solution.py:258
  275.8 22.0 %all_gather.74 = bf16[1024,128]{1,0:T(8,128)(2,1)S(1)} all-gather(bf16[32,128]{1,0:T(8,128)(2,1)S(1)} %copy-done.4), channel_id=1, replica_groups=mesh['sp'=32,'tp'=4] {'sp'}, dimensions={0}, use_global_device_ids=true | all-gather | bytes 270336 | tf_op jit(solution)/shard_map/all_gather | solution.py:264
  298.3 24.7 %all_gather.75 = bf16[256,1024]{0,1:T(8,128)(2,1)S(1)} all-gather(bf16[256,32]{0,1:T(8,128)(2,1)S(1)} %pad_maximum_fusion.2), channel_id=1, replica_groups=mesh['sp'=32,'tp'=4] {'sp'}, dimensions={1}, use_global_device_ids=true | all-gather | bytes 540672 | tf_op jit(solution)/shard_map/all_gather | solution.py:303
  323.9 33.5 %while.74 = (s32[]{:T(128)}, f32[2,64,64]{2,1,0:T(8,128)S(1)}, s32[]{:T(128)}, f32[32,2,64,64]{3,2,1,0:T(8,128)}, f32[32,2,64,64]{3,2,1,0:T(8,128)}, /*index=5*/s32[]{:T(128)}, s32[]{:T(128)}, s32[]{:T(128)}, s32[]{:T(128)}) while((s32[]{:T(128)}, f32[2,64,64]{2,1,0:T(8,128)S(1)}, s32[]{:T(128)}, f32[32,2,64,64]{3,2,1,0:T(8,128)}, ...), condition=%wide.region_16.18_spmd, body=%wide.region_15.17_spmd.sunk | while | flops 6299654 | bytes 263307 | solution.py:28
  323.9 1.1 convolution_add_fusion.18
  325.0 1.1 convolution_add_fusion.18
  326.2 1.1 convolution_add_fusion.18
  327.3 1.1 convolution_add_fusion.18
  328.4 1.1 convolution_add_fusion.18
  329.5 1.1 convolution_add_fusion.18
  330.6 1.1 convolution_add_fusion.18
  331.7 1.1 convolution_add_fusion.18
  332.9 1.1 convolution_add_fusion.18
  334.0 1.1 convolution_add_fusion.18
  335.1 1.1 convolution_add_fusion.18
  336.2 1.1 convolution_add_fusion.18
  337.3 1.1 convolution_add_fusion.18
  338.4 1.1 convolution_add_fusion.18
  339.6 1.1 convolution_add_fusion.18
  340.7 1.1 convolution_add_fusion.18
  341.8 1.1 convolution_add_fusion.18
  342.9 1.1 convolution_add_fusion.18
  344.0 1.1 convolution_add_fusion.18
  346.2 1.1 convolution_add_fusion.18
  348.5 1.1 convolution_add_fusion.18
  350.7 1.1 convolution_add_fusion.18
  357.4 3.6 while.75
  361.2 8.6 %all-gather.13.cloned.1.call-done = f32[64,64,64]{2,1,0:T(8,128)} async-done(((f32[2,64,64]{2,1,0:T(8,128)}), f32[64,64,64]{2,1,0:T(8,128)}) %all-gather.13.cloned.1.call-update) | async-done | bytes 1048592 | tf_op jit(solution)/shard_map/all_gather | solution.py:19
  369.8 1.1 while.71
  369.8 1.1 convolution_add_fusion.15
  371.0 3.6 while.72
  374.8 1.1 fusion.107
  375.9 50.5 %reduce-scatter.2.cloned.1.call-done = f32[32,1024]{1,0:T(8,128)} async-done(((f32[128,1024]{1,0:T(8,128)}), f32[32,1024]{1,0:T(8,128)}) %reduce-scatter.2.cloned.1.call-update) | async-done | bytes 131088 | tf_op jit(solution)/shard_map/reduce_scatter | solution.py:314
  426.4 1.5 convert_element_type.96
  (259 shorter events, 35.2 us)
Async XLA Ops:
  6.5 66.0 %copy-start.14 = (f32[1024]{0:T(1024)S(1)}, f32[1024]{0:T(1024)}, u32[]{:S(2)}) copy-start(f32[1024]{0:T(1024)} %param.32) | copy-start | bytes 12292
  6.5 66.9 %copy-start = (bf16[32,128]{1,0:T(8,128)(2,1)S(1)}, bf16[32,128]{1,0:T(8,128)(2,1)}, u32[]{:S(2)}) copy-start(bf16[32,128]{1,0:T(8,128)(2,1)} %param.39) | copy-start | bytes 24580
  6.5 317.3 %all-gather.15.cloned.1.call-start = ((), (), s32[]{:S(2)}) async-start(), calls=%async_computation.4 | async-start | bytes 2162688 | tf_op jit(solution)/shard_map/all_gather | solution.py:19
  47.2 49.2 %copy-start.8 = (bf16[32,2,2]{0,2,1:T(2,128)(2,1)S(1)}, bf16[32,2,2]{0,2,1:T(2,128)(2,1)}, u32[]{:S(2)}) copy-start(bf16[32,2,2]{0,2,1:T(2,128)(2,1)} %param.42) | copy-start | bytes 772
  48.2 72.3 %copy-start.10 = (f32[2,2]{1,0:T(2,128)S(1)}, f32[2,2]{1,0:T(2,128)}, u32[]{:S(2)}) copy-start(f32[2,2]{1,0:T(2,128)} %param.44) | copy-start | bytes 52
  72.5 49.8 %copy-start.9 = (bf16[32,2,2]{0,2,1:T(2,128)(2,1)S(1)}, bf16[32,2,2]{0,2,1:T(2,128)(2,1)}, u32[]{:S(2)}) copy-start(bf16[32,2,2]{0,2,1:T(2,128)(2,1)} %param.41) | copy-start | bytes 772
  73.0 71.7 %copy-start.11 = (f32[2,2]{1,0:T(2,128)S(1)}, f32[2,2]{1,0:T(2,128)}, u32[]{:S(2)}) copy-start(f32[2,2]{1,0:T(2,128)} %param.43) | copy-start | bytes 52
  145.3 42.7 %copy-start.13 = (pred[128]{0:T(512)(128)(4,1)S(1)}, pred[128]{0:T(512)(128)(4,1)}, u32[]{:S(2)}) copy-start(pred[128]{0:T(512)(128)(4,1)} %constant.168.clone.1) | copy-start | bytes 388
  190.8 4.6 %copy-start.1 = (bf16[32,64]{1,0:T(8,128)(2,1)S(1)}, bf16[32,64]{1,0:T(8,128)(2,1)}, u32[]{:S(2)}) copy-start(bf16[32,64]{1,0:T(8,128)(2,1)} %param.35) | copy-start | bytes 12292
  190.8 28.9 %copy-start.2 = (bf16[32,64]{1,0:T(8,128)(2,1)S(1)}, bf16[32,64]{1,0:T(8,128)(2,1)}, u32[]{:S(2)}) copy-start(bf16[32,64]{1,0:T(8,128)(2,1)} %param.34) | copy-start | bytes 12292
  191.5 132.4 %all-gather.17.cloned.1.call-start = ((), (), s32[]{:S(2)}) async-start(), calls=%async_computation.5 | async-start | bytes 2162688 | tf_op jit(solution)/shard_map/all_gather | solution.py:19
  192.3 168.9 %all-gather.11.cloned.1.call-start = ((), (), s32[]{:S(2)}) async-start(), calls=%async_computation.2 | async-start | bytes 2162688 | tf_op jit(solution)/shard_map/all_gather | solution.py:19
  194.6 54.0 %copy-start.3 = (bf16[32,128]{1,0:T(8,128)(2,1)S(1)}, bf16[32,128]{1,0:T(8,128)(2,1)}, u32[]{:S(2)}) copy-start(bf16[32,128]{1,0:T(8,128)(2,1)} %param.33) | copy-start | bytes 24580
  194.6 81.3 %copy-start.4 = (bf16[32,128]{1,0:T(8,128)(2,1)S(1)}, bf16[32,128]{1,0:T(8,128)(2,1)}, u32[]{:S(2)}) copy-start(bf16[32,128]{1,0:T(8,128)(2,1)} %param.40) | copy-start | bytes 24580
  195.3 174.5 %all-gather.13.cloned.1.call-start = ((), (), s32[]{:S(2)}) async-start(), calls=%async_computation.3 | async-start | bytes 2162688 | tf_op jit(solution)/shard_map/all_gather | solution.py:19
  242.1 56.1 %copy-start.5 = (bf16[128,32]{0,1:T(8,128)(2,1)S(1)}, bf16[128,32]{0,1:T(8,128)(2,1)}, u32[]{:S(2)}) copy-start(bf16[128,32]{0,1:T(8,128)(2,1)} %param.47) | copy-start | bytes 24580
  242.1 56.1 %copy-start.6 = (bf16[128,32]{0,1:T(8,128)(2,1)S(1)}, bf16[128,32]{0,1:T(8,128)(2,1)}, u32[]{:S(2)}) copy-start(bf16[128,32]{0,1:T(8,128)(2,1)} %param.46) | copy-start | bytes 24580
  242.7 80.3 %collective-permute-start = (bf16[64,128]{0,1:T(8,128)(2,1)S(1)}, bf16[64,128]{0,1:T(8,128)(2,1)S(1)}, u32[]{:S(2)}, u32[]{:S(2)}) collective-permute-start(bf16[64,128]{0,1:T(8,128)(2,1)S(1)} %get-tuple-element.542), channel_id=1, source_target_pairs={{0,4},{4,8},{8,12},{12,16},{16,20},{20,24},{24,28},{28,32},{32,36}... | collective-permute-start | bytes 49160 | tf_op jit(solution)/shard_map/ppermute | solution.py:39
  245.7 77.4 %collective-permute-start.1 = (bf16[64,128]{0,1:T(8,128)(2,1)S(1)}, bf16[64,128]{0,1:T(8,128)(2,1)S(1)}, u32[]{:S(2)}, u32[]{:S(2)}) collective-permute-start(bf16[64,128]{0,1:T(8,128)(2,1)S(1)} %get-tuple-element.543), channel_id=1, source_target_pairs={{4,0},{8,4},{12,8},{16,12},{20,16},{24,20},{28,24},{32,28},{36,32}... | collective-permute-start | bytes 49160 | tf_op jit(solution)/shard_map/ppermute | solution.py:41
  247.6 178.8 %reduce-scatter.2.cloned.1.call-start = ((), (), s32[]{:S(2)}) async-start(), calls=%async_computation.1 | async-start | bytes 655360 | tf_op jit(solution)/shard_map/reduce_scatter | solution.py:314
  247.7 75.7 %copy-start.7 = (f32[2]{0:T(128)S(1)}, f32[2]{0:T(128)}, u32[]{:S(2)}) copy-start(f32[2]{0:T(128)} %param.36) | copy-start | bytes 28
  370.9 3.8 copy-start.12
Sparse Core Ops, SparseCore 0:
  191.6 42.2 all-gather.14
  236.2 42.8 all-gather.16
  281.4 43.4 all-gather.10
  327.0 42.8 all-gather.12
  376.1 50.3 reduce-scatter.1
where the time goes:
time: 438 us; the launch traced here: 434 us
  blocking collectives  253 us (58%)
  waiting for transfers between devices  59.9 us (14%)
  matrix products  51.1 us (12%)
  other arithmetic  44.5 us (10%)
  between operations  13.9 us (3%)
  local copies, waits for them, and re-layouts  5.38 us (1%)
  starting transfers between devices  5.02 us (1%)
    reduce_scatter x1, waiting for transfers between devices, per_device(): lax.psum_scatter(term_rows(), 'tp', scatter_dimension=0, tiled=True)  50.5 us
    another operation x4, other arithmetic, block_pass(): lax.linalg.triangular_solve(system, right_side, left_side=True, lower=Tru...  39.5 us
    dot_general x31, matrix products, compose(): jnp.einsum('hij,hjk->hik', later_map[0], earlier_map[1], precision=highest)  33.1 us
    all_gather x1, blocking collectives, per_device(): lax.all_gather(delta_key, 'sp', axis=0, tiled=True)  29.1 us
    all_gather x1, blocking collectives, per_device(): lax.all_gather(attn_query, 'sp', axis=0, tiled=True)  27 us
    all_gather x1, blocking collectives, per_device(): full_weight = lax.all_gather(stacked, 'sp', axis=1, tiled=True)  24.7 us
    all_gather x1, blocking collectives, per_device(): lax.all_gather(attn_value, 'sp', axis=0, tiled=True)  24.3 us
    all_gather x1, blocking collectives, per_device(): lax.all_gather(delta_query, 'sp', axis=0, tiled=True)  24.1 us
  transfers between devices with their start and end apart: 7, of which 2 were waited for; matrix products, arithmetic and copies ran while one was open for 10% of the time, Pallas kernels for 0%

commit v1 on v0

v1 whole, which is shorter than its diff:
```python
import jax
import jax.numpy as jnp
from jax import lax
from jax.experimental import pallas as pl
from jax.experimental.pallas import tpu as pltpu
from jax.sharding import PartitionSpec as P

HEAD_DIM = 64
WINDOW = 64
ROWS = 256
TOKENS = 4096
EPS = 1e-6
COPIES = 96
MESH = pl.DeviceIdType.MESH
F32 = jnp.float32
BF16 = jnp.bfloat16
NN = (((1,), (0,)), ((), ()))
NT = (((1,), (1,)), ((), ()))


def mm(a, b, dims=NN):
    return lax.dot_general(a, b, dims, preferred_element_type=F32)


def split(a):
    hi = a.astype(BF16)
    return hi, (a - hi.astype(F32)).astype(BF16)


def dot3(a, b):
    ah, al = split(a)
    bh, bl = split(b)
    return mm(ah, bh) + (mm(ah, bl) + mm(al, bh))


def dot3_deep(a, b):
    ah, al = split(a)
    bh, bl = split(b)
    return mm(jnp.concatenate([ah, ah, al], axis=1), jnp.concatenate([bh, bl, bh], axis=0))


def silu(v):
    return v * jax.nn.sigmoid(v)


def inverse(low, same):
    eye = jnp.where(same(0), 1.0, 0.0)
    d1 = jnp.where(same(4), low, 0.0)
    d2 = dot3(d1, d1)
    x = eye - d1
    x = x + dot3(x, d2)
    d4 = dot3(d2, d2)
    x = x + dot3(x, d4)
    d8 = dot3(d4, d4)
    x = x + dot3(x, d8)
    for k in range(4, 8):
        off = jnp.where(same(k + 1), low, 0.0) - jnp.where(same(k), low, 0.0)
        x = x - dot3(dot3(x, off), x)
    return x


def layer_kernel(
    tokens, gain, aq, ak, av, dq, dk, dv, dz, small, ogain, ao, do, sink, shift, dlog,
    out,
    tok, normed, stage, w1, w2, kv, mats, rowmats, hsend, hall, pbuf, prec, send_sem, recv_sem, own_sem,
):
    sp = lax.axis_index("sp")
    x = lax.axis_index("tp")
    c = lax.rem(sp, 2)
    b = lax.div(sp, 2)
    z = lax.div(b, 4)
    y = lax.rem(b, 4)
    o = 1 - c

    def m4(v):
        return lax.rem(v + 4, 4)

    def dev(zz, yy, cc, xx):
        return {"sp": (zz * 4 + yy) * 2 + cc, "tp": xx}

    def dev_x(d):
        return dev(z, y, c, m4(x + d))

    def dev_y(d):
        return dev(z, m4(y + d), c, x)

    def dev_z(d):
        return dev(m4(z + d), y, c, x)

    def dev_b(d):
        bb = lax.rem(b + d + 16, 16)
        return {"sp": bb * 2 + c, "tp": x}

    partner = dev(z, y, o, x)
    sent = []

    def send(src, dst, device, landed):
        i = len(sent)
        copy = pltpu.make_async_remote_copy(
            src_ref=src, dst_ref=dst, send_sem=send_sem.at[i], recv_sem=recv_sem.at[i],
            device_id=device, device_id_type=MESH,
        )
        copy.start()
        sent.append(copy)
        return pltpu.make_async_remote_copy(
            src_ref=landed, dst_ref=landed, send_sem=send_sem.at[i], recv_sem=recv_sem.at[i],
            device_id=device, device_id_type=MESH,
        )

    attn_t = ao[...].astype(F32).T.astype(BF16)
    delta_t = do[...].astype(F32).T.astype(BF16)
    for cc in range(2):
        cols = slice(64 * cc, 64 * cc + 64)
        stage[cc] = jnp.concatenate(
            [aq[:, cols], dq[:, cols], dk[:, cols], dv[:, cols], dz[:, cols], small[cc], ak[...], av[...],
             attn_t[:, cols], delta_t[:, cols]],
            axis=1,
        )
    w1[z, y, c] = stage[c, :, 0:512]

    barrier = pltpu.get_barrier_semaphore()
    peers = [partner]
    for d in (1, 2, 3):
        peers += [dev_x(d), dev_y(d), dev_z(d)]
    peers += [dev_b(1), dev_b(-1)]
    for peer in peers:
        pl.semaphore_signal(barrier, inc=1, device_id=peer, device_id_type=MESH)
    pl.semaphore_wait(barrier, len(peers))

    class Ring:
        def __init__(self, w, s, y_first):
            self.w, self.s, self.y_first = w, s, y_first

        def slot(self, first, half=None):
            zz, yy = (z, m4(y + first)) if self.y_first else (m4(z + first), y)
            ref = self.w.at[zz, yy, self.s]
            return ref if half is None else ref.at[pl.ds(16 * half, 16)]

        def line(self, second, half=None):
            rows = pl.ds(0, 32) if half is None else pl.ds(16 * half, 16)
            if self.y_first:
                return self.w.at[m4(z + second), :, self.s, rows]
            return self.w.at[:, m4(y + second), self.s, rows]

        def dev1(self, d):
            return dev_y(d) if self.y_first else dev_z(d)

        def dev2(self, d):
            return dev_z(d) if self.y_first else dev_y(d)

        def start1(self):
            self.up = send(self.slot(0), self.slot(0), self.dev1(1), self.slot(-1))
            self.down = send(self.slot(0), self.slot(0), self.dev1(-1), self.slot(1))

        def relay1(self):
            self.up.wait_recv()
            self.up2 = send(self.slot(-1, 0), self.slot(-1, 0), self.dev1(1), self.slot(-2, 0))
            self.down.wait_recv()
            self.down2 = send(self.slot(1, 1), self.slot(1, 1), self.dev1(-1), self.slot(2, 1))

        def start2(self):
            self.up2.wait_recv()
            self.down2.wait_recv()
            self.up = send(self.line(0), self.line(0), self.dev2(1), self.line(-1))
            self.down = send(self.line(0), self.line(0), self.dev2(-1), self.line(1))

        def relay2(self):
            self.up.wait_recv()
            self.up2 = send(self.line(-1, 0), self.line(-1, 0), self.dev2(1), self.line(-2, 0))
            self.down.wait_recv()
            self.down2 = send(self.line(1, 1), self.line(1, 1), self.dev2(-1), self.line(2, 1))

        def finish(self):
            self.up2.wait_recv()
            self.down2.wait_recv()

    half_rows = pl.ds(128 * c, 128)
    other_rows = pl.ds(128 * o, 128)
    in_cols = pl.ds(0, 512)
    out_cols = pl.ds(512, 128)
    x_cols = pl.ds(pl.multiple_of(128 * x, 128), 128)

    def x_cols_of(d):
        return pl.ds(pl.multiple_of(128 * m4(x + d), 128), 128)

    w_swap = send(stage.at[o, :, in_cols], w1.at[z, y, c], partner, w1.at[z, y, o])
    first = Ring(w1, c, True)
    second = Ring(w1, o, False)
    first.start1()
    tok_in = [send(tokens, tok.at[x, half_rows], dev_x(d), tok.at[m4(x - d), half_rows]) for d in (1, 3, 2)]
    tok_swap = [send(tokens, tok.at[x, half_rows], partner, tok.at[x, other_rows])]
    w2_swap = send(stage.at[o, :, out_cols], w2.at[z, y, c, :, x_cols], partner, w2.at[z, y, o, :, x_cols])
    own_tok = pltpu.make_async_copy(tokens, tok.at[x, half_rows], own_sem.at[0])
    own_tok.start()
    own_w2 = pltpu.make_async_copy(stage.at[c, :, out_cols], w2.at[z, y, c, :, x_cols], own_sem.at[1])
    own_w2.start()
    w_swap.wait_recv()
    second.start1()
    first.relay1()
    second.relay1()
    for d, arrived in zip((1, 3, 2), tok_in):
        arrived.wait_recv()
        src = m4(x - d)
        tok_swap.append(send(tok.at[src, half_rows], tok.at[src, half_rows], partner, tok.at[src, other_rows]))
    first.start2()
    second.start2()
    own_w2.wait()
    w2_swap.wait_recv()
    w2_in = [
        send(w2.at[z, y, :, :, x_cols], w2.at[z, y, :, :, x_cols], dev_x(d), w2.at[z, y, :, :, x_cols_of(-d)])
        for d in (1, 3, 2)
    ]
    own_tok.wait()
    for arrived in tok_swap:
        arrived.wait_recv()

    squares = jnp.zeros((ROWS, 1), F32)
    for k in range(4):
        wide = tok[k].astype(F32)
        squares = squares + jnp.sum(wide * wide, axis=-1, keepdims=True)
    inv = lax.rsqrt(squares * (1.0 / 1024.0) + EPS)
    for k in range(4):
        normed[k] = (tok[k].astype(F32) * inv * gain[:, 256 * k : 256 * k + 256]).astype(BF16)

    first.relay2()
    second.relay2()
    first.finish()
    second.finish()
    for arrived in w2_in:
        arrived.wait_recv()
    out_first = Ring(w2, c, True)
    out_second = Ring(w2, o, False)
    out_first.start1()
    out_second.start1()

    proj = mm(normed[0], w1[0].reshape(256, 512))
    for k in range(1, 4):
        proj = proj + mm(normed[k], w1[k].reshape(256, 512))
    t0, t1, t2 = proj[:, 0:128], proj[:, 128:256], proj[:, 256:384]
    kv[64:320, :] = proj[:, 384:512].astype(BF16)
    halo = [
        send(kv.at[pl.ds(256, 64)], kv.at[pl.ds(0, 64)], dev_b(1), kv.at[pl.ds(0, 64)]),
        send(kv.at[pl.ds(64, 64)], kv.at[pl.ds(320, 64)], dev_b(-1), kv.at[pl.ds(320, 64)]),
    ]
    att_q = t0[:, 0:64].astype(BF16)
    act_q = silu(t0[:, 64:128].astype(BF16).astype(F32))
    act_kv = silu(t1.astype(BF16).astype(F32))
    act_k, val = act_kv[:, 0:64], act_kv[:, 64:128]
    q = act_q * lax.rsqrt(jnp.sum(act_q * act_q, axis=-1, keepdims=True) + EPS) * HEAD_DIM**-0.5
    key = act_k * lax.rsqrt(jnp.sum(act_k * act_k, axis=-1, keepdims=True) + EPS)
    gate = silu(t2[:, 0:64].astype(BF16).astype(F32))

    lane = lax.broadcasted_iota(jnp.int32, (1, 128), 1)
    bias = jnp.where(lane == 64, shift[0, c], jnp.where(lane == 65, shift[1, c], 0.0))
    rate = jnp.exp(jnp.where(lane == 66, dlog[0, c], jnp.where(lane == 67, dlog[1, c], 0.0)))
    strength = jax.nn.sigmoid(t2 + bias)
    softplus = jnp.maximum(t2, 0.0) + jnp.log1p(jnp.exp(-jnp.abs(t2)))
    decay = jnp.where((lane == 66) | (lane == 67), -rate * softplus * (1.0 / TOKENS), 0.0)

    row = lax.broadcasted_iota(jnp.int32, (ROWS, ROWS), 0)
    col = lax.broadcasted_iota(jnp.int32, (ROWS, ROWS), 1)
    lower = row >= col
    upper = row <= col

    def same(k):
        return lax.shift_right_logical(row, k) == lax.shift_right_logical(col, k)

    g_hi = decay.astype(BF16)
    rest = decay - g_hi.astype(F32)
    g_mid = rest.astype(BF16)
    g_lo = (rest - g_mid.astype(F32)).astype(BF16)
    g_parts = jnp.concatenate([g_hi[:, 64:128], g_mid[:, 64:128], g_lo[:, 64:128]], axis=1)
    both = []
    for mask in (lower, upper):
        s = mm(jnp.where(mask, 1.0, 0.0).astype(BF16), g_parts)
        both.append(s[:, 0:64] + s[:, 64:128] + s[:, 128:192])
    sub = lax.broadcasted_iota(jnp.int32, (1, 64), 1)
    g_all = jnp.where(sub == 2, both[0], both[1])
    turned = jnp.concatenate([key, g_all], axis=1).T
    key_t = turned[0:64]
    key_h, key_l = split(key)
    q_h, q_l = split(q)
    kt_h, kt_l = split(key_t)
    pairs = mm(
        jnp.concatenate(
            [jnp.concatenate([q_h, q_h, q_l], axis=1), jnp.concatenate([key_h, key_h, key_l], axis=1)], axis=0
        ),
        jnp.concatenate([kt_h, kt_l, kt_h], axis=0),
    )
    qk, kk = pairs[0:ROWS], pairs[ROWS:]

    lane2 = lax.broadcasted_iota(jnp.int32, (64, 128), 1)
    row2 = lax.broadcasted_iota(jnp.int32, (64, 128), 0)
    eye2 = jnp.where(lane2 == row2 + 64, 1.0, 0.0)
    local, reads = [], []
    for way, mask in ((0, lower), (1, upper)):
        beta = strength[:, 64 + way : 65 + way]
        g_col = g_all[:, 2 + way : 3 + way]
        g_row = turned[66 + way : 67 + way]
        g_end = g_col[ROWS - 1 : ROWS] if way == 0 else g_col[0:1]
        decays = jnp.exp(jnp.where(mask, g_col - g_row, -jnp.inf))
        low = jnp.where(row == col, 0.0, beta * kk * decays)
        t_inv = inverse(low, same)
        grown = jnp.exp(g_col)
        uw = dot3(t_inv, jnp.concatenate([beta * val, (beta * grown) * key], axis=1))
        read = dot3(qk * decays, uw)
        local.append(read[:, 0:64])
        reads.append(grown * q - read[:, 64:128])
        final = dot3(key_t * jnp.exp(g_end - g_row), uw)
        mats[y, way] = jnp.where(lane2 < 64, final, jnp.exp(g_end) * eye2 - final)
    scan1 = [send(mats.at[y], mats.at[y], dev_y(d), mats.at[m4(y - d)]) for d in (1, 3, 2)]

    out_first.relay1()
    out_second.relay1()

    for arrived in halo:
        arrived.wait_recv()
    scores = mm(att_q, kv[:, 0:64], NT) * HEAD_DIM**-0.5
    q_pos = lax.broadcasted_iota(jnp.int32, (ROWS, ROWS + 2 * WINDOW), 0)
    k_pos = lax.broadcasted_iota(jnp.int32, (ROWS, ROWS + 2 * WINDOW), 1) - WINDOW
    seen = k_pos + b * ROWS
    allowed = (jnp.abs(q_pos - k_pos) <= WINDOW) & (seen >= 0) & (seen < TOKENS)
    scores = jnp.where(allowed, scores, -jnp.inf)
    top = jnp.maximum(jnp.max(scores, axis=-1, keepdims=True), sink[c])
    weights = jnp.exp(scores - top)
    total = jnp.sum(weights, axis=-1, keepdims=True) + jnp.exp(sink[c] - top)
    weights = (weights / total).astype(BF16)
    attn_heads = mm(weights, kv[:, 64:128])

    out_first.start2()
    out_second.start2()

    for arrived in scan1:
        arrived.wait_recv()

    def after(later, earlier):
        return dot3_deep(later[:, 64:128], earlier) + jnp.where(lane2 < 64, later, 0.0)

    entry = []
    for way in range(2):
        m = [mats[k if way == 0 else 3 - k, way] for k in range(4)]
        place = y if way == 0 else 3 - y
        two = after(m[1], m[0])
        three = after(m[2], two)
        rowmats[z, way] = after(after(m[3], m[2]), two)
        entry.append(
            jnp.where(place == 0, eye2, jnp.where(place == 1, m[0], jnp.where(place == 2, two, three)))
        )
    scan2 = [send(rowmats.at[z], rowmats.at[z], dev_z(d), rowmats.at[m4(z - d)]) for d in (1, 3, 2)]
    out_first.relay2()
    out_second.relay2()
    for arrived in scan2:
        arrived.wait_recv()
    states = []
    for way in range(2):
        m = [rowmats[k if way == 0 else 3 - k, way] for k in range(3)]
        place = z if way == 0 else 3 - z
        s1 = m[0][:, 0:64]
        s2 = dot3_deep(m[1][:, 64:128], s1) + m[1][:, 0:64]
        s3 = dot3_deep(m[2][:, 64:128], s2) + m[2][:, 0:64]
        s = jnp.where(place == 0, 0.0, jnp.where(place == 1, s1, jnp.where(place == 2, s2, s3)))
        states.append(dot3_deep(entry[way][:, 64:128], s) + entry[way][:, 0:64])

    whole = local[0] + local[1] + dot3(jnp.concatenate(reads, axis=1), jnp.concatenate(states, axis=0))
    scaled = whole * lax.rsqrt(jnp.mean(whole * whole, axis=-1, keepdims=True) + EPS) * ogain[...]
    heads = jnp.concatenate([attn_heads, scaled * gate], axis=1).astype(BF16)
    for k in range(4):
        hsend[k, 0:32] = heads[32 * k : 32 * k + 32]
        hsend[k, 32:64] = heads[128 + 32 * k : 160 + 32 * k]
    head_in = [send(hsend.at[m4(x + d)], hall.at[x], dev_x(d), hall.at[m4(x - d)]) for d in (1, 3, 2)]
    hall[x] = hsend[x]
    out_first.finish()
    out_second.finish()
    for arrived in head_in:
        arrived.wait_recv()
    gathered = jnp.concatenate([hall[k] for k in range(4)], axis=1)
    for k in range(4):
        part = mm(gathered, w2[k].reshape(256, 512), NT)
        pbuf[0, :, 256 * k : 256 * k + 256] = part[0:32]
        pbuf[1, :, 256 * k : 256 * k + 256] = part[32:64]
    last = send(pbuf.at[o], prec, partner, prec)
    last.wait_recv()
    out[...] = (pbuf[c] + prec[...]).astype(BF16)
    for copy in sent:
        copy.wait_send()


def per_device(
    tokens, norm_gain, attn_query, attn_key, attn_value, sink_logit, delta_query, delta_key, delta_value,
    delta_gate, beta_weight, decay_weight, beta_shift, decay_log, out_gain, attn_out, delta_out,
):
    small = jnp.concatenate([beta_weight, decay_weight], axis=2).transpose(1, 0, 2)
    small = jnp.pad(small, ((0, 0), (0, 0), (0, 60)))
    vmem = pl.BlockSpec(memory_space=pltpu.VMEM)
    smem = pl.BlockSpec(memory_space=pltpu.SMEM)
    return pl.pallas_call(
        layer_kernel,
        out_shape=jax.ShapeDtypeStruct((32, 1024), BF16),
        in_specs=[vmem] * 13 + [smem] * 3,
        out_specs=vmem,
        scratch_shapes=[
            pltpu.VMEM((4, 256, 256), BF16),
            pltpu.VMEM((4, 256, 256), BF16),
            pltpu.VMEM((2, 32, 640), BF16),
            pltpu.VMEM((4, 4, 2, 32, 512), BF16),
            pltpu.VMEM((4, 4, 2, 32, 512), BF16),
            pltpu.VMEM((384, 128), BF16),
            pltpu.VMEM((4, 2, 64, 128), F32),
            pltpu.VMEM((4, 2, 64, 128), F32),
            pltpu.VMEM((4, 64, 128), BF16),
            pltpu.VMEM((4, 64, 128), BF16),
            pltpu.VMEM((2, 32, 1024), F32),
            pltpu.VMEM((32, 1024), F32),
            pltpu.SemaphoreType.DMA((COPIES,)),
            pltpu.SemaphoreType.DMA((COPIES,)),
            pltpu.SemaphoreType.DMA((2,)),
        ],
        compiler_params=pltpu.CompilerParams(collective_id=0, has_side_effects=True),
    )(
        tokens, norm_gain.reshape(1, -1), attn_query, attn_key, attn_value, delta_query, delta_key, delta_value,
        delta_gate, small, out_gain.reshape(1, -1), attn_out, delta_out, sink_logit, beta_shift, decay_log,
    )


def solution(mesh):
    return jax.shard_map(
        per_device,
        mesh=mesh,
        in_specs=(
            P("sp", "tp"), P(), P("sp", "tp"), P("sp", "tp"), P("sp", "tp"), P("tp"), P("sp", "tp"),
            P("sp", "tp"), P("sp", "tp"), P("sp", "tp"), P("sp", "tp", None), P("sp", "tp", None),
            P(None, "tp"), P(None, "tp"), P(), P("tp", "sp"), P("tp", "sp"),
        ),
        out_specs=P(("sp", "tp"), None),
        check_vma=False,
    )
```

time: 438 us -> 60.3 us (0.14)
  blocking collectives: 253 us -> 0 us
  waiting for transfers between devices: 59.9 us -> 0 us
  Pallas kernels: 0 us -> 55.6 us
  matrix products: 51.1 us -> 0 us
  other arithmetic: 44.5 us -> 0.01 us
  between operations: 13.9 us -> 0.02 us
  starting transfers between devices: 5.02 us -> 0 us
    all_gather x11 -> x0, blocking collectives: 253 us -> none  [the longest x1 29.1 us: per_device(): lax.all_gather(delta_key, 'sp', axis=0, tiled=True)]
    pallas_call x0 -> x1, Pallas kernels: none -> 55.6 us  [per_device(): pl.pallas_call(layer_kernel, out_shape=jax.ShapeDtypeStruct((32, 1024), B...]
    reduce_scatter x1 -> x0, waiting for transfers between devices: 50.5 us -> none  [per_device(): lax.psum_scatter(term_rows(), 'tp', scatter_dimension=0, tiled=True)]
    dot_general x95 -> x0, matrix products: 50.2 us -> none  [the longest x31 33.1 us: compose(): jnp.einsum('hij,hjk->hik', later_map[0], earlier_map[1], precision=highest)]
    another operation x6 -> x0, other arithmetic: 41.1 us -> none  [the longest x4 39.5 us: block_pass(): lax.linalg.triangular_solve(system, right_side, left_side=True, lower=Tru...]
    all_gather x4 -> x0, waiting for transfers between devices: 8.68 us -> none  [prefix(): gathered = jax.tree.map(lambda a: lax.all_gather(a, axis), part)]
    ppermute x2 -> x0, starting transfers between devices: 4.85 us -> none  [the longest x1 2.93 us: extended(): lax.ppermute(tail, axis, [(i, (i + 1) % count) for i in range(ends)])]
  transfers between devices with their start and end apart: 7 -> 0, of which waited for: 2 -> 0; matrix products, arithmetic and copies ran while one was open for 10% -> 0% of each run, Pallas kernels for 0% -> 0%
where the time goes in v1:
time: 60.3 us; the launch traced here: 60 us
  Pallas kernels  55.6 us (92%)
  local copies, waits for them, and re-layouts  4.41 us (7%)
    pallas_call x1, Pallas kernels, per_device(): pl.pallas_call(layer_kernel, out_shape=jax.ShapeDtypeStruct((32, 1024), B...  55.6 us
    unnamed x11, local copies, waits for them, and re-layouts  3.7 us

profile of v1, /device:TPU:1, one launch (start us, length us, event | category | flops | bytes accessed | tf_op | source)
XLA Modules:
  0.0 60.0 jit_solution(5996391096997610475)
XLA Ops:
  0.0 0.0 copy-start.3
  0.0 0.0 copy-start.2
  0.0 0.7 %copy-done.3 = bf16[32,2,2]{0,2,1:T(2,128)(2,1)S(1)} copy-done((bf16[32,2,2]{0,2,1:T(2,128)(2,1)S(1)}, bf16[32,2,2]{0,2,1:T(2,128)(2,1)}, u32[]{:S(2)}) %copy-start.3) | copy-done | bytes 280
  0.7 0.0 copy-done.2
  0.7 0.1 copy.22
  0.8 0.0 copy-start
  0.8 0.6 %pad.4.small = bf16[2,32,64]{2,1,0:T(8,128)(2,1)} pad(bf16[2,32,4]{2,1,0:T(8,128)(2,1)S(1)} %bitcast.3, bf16[]{:T(256)} %constant.2.clone.1), padding=0_0x0_0x0_60 | pad | bytes 8706 | tf_op jit(solution)/shard_map/jit(_pad)/pad | solution.py:393
  1.4 0.1 copy-done
  1.5 0.0 copy-start.1
  1.5 0.7 %copy.23.ao = bf16[128,32]{1,0:T(8,128)(2,1)} copy(bf16[128,32]{0,1:T(8,128)(2,1)S(1)} %copy-done) | data formatting | bytes 16384 | tf_op args[15]
  2.2 0.0 copy-done.1
  2.3 0.7 %copy.24.do = bf16[128,32]{1,0:T(8,128)(2,1)} copy(bf16[128,32]{0,1:T(8,128)(2,1)S(1)} %copy-done.1) | data formatting | bytes 16384 | tf_op args[16]
  3.0 55.6 %shard_map.163 = bf16[32,1024]{1,0:T(8,128)(2,1)} custom-call(bf16[128,256]{1,0:T(8,128)(2,1)} %tokens.1, f32[1,1024]{1,0:T(1,128)} %bitcast.4, bf16[32,128]{1,0:T(8,128)(2,1)} %aq.1, bf16[32,64]{1,0:T(8,128)(2,1)} %ak.1, bf16[32,64]{1,0:T(8,128)(2,1)} %av.1, bf16[32,128]{1,0:T(8,128)(2,1)} %dq.1, bf16[32,128]{1,0:T(8,128)(2,1)} %dk.1, bf16[32,128]{1,0:T(8,128)(2,1)} %dv.1, ...), custom_call_target="tpu_custom_call" | custom-call | tf_op jit(solution)/shard_map/pallas_call | solution.py:396
  58.6 1.5 %copy.26 = bf16[32,1024]{1,0:T(8,128)(2,1)} copy(bf16[32,1024]{1,0:T(8,128)(2,1)} %shard_map.163) | data formatting | bytes 131072
  (1 shorter events, 0.0 us)
Async XLA Ops:
  0.0 0.7 %copy-start.3 = (bf16[32,2,2]{0,2,1:T(2,128)(2,1)S(1)}, bf16[32,2,2]{0,2,1:T(2,128)(2,1)}, u32[]{:S(2)}) copy-start(bf16[32,2,2]{0,2,1:T(2,128)(2,1)} %param.27) | copy-start | bytes 772
  0.0 0.7 %copy-start.2 = (bf16[32,2,2]{0,2,1:T(2,128)(2,1)S(1)}, bf16[32,2,2]{0,2,1:T(2,128)(2,1)}, u32[]{:S(2)}) copy-start(bf16[32,2,2]{0,2,1:T(2,128)(2,1)} %param.28) | copy-start | bytes 772
  0.8 0.7 %copy-start = (bf16[128,32]{0,1:T(8,128)(2,1)S(1)}, bf16[128,32]{0,1:T(8,128)(2,1)}, u32[]{:S(2)}) copy-start(bf16[128,32]{0,1:T(8,128)(2,1)} %param.32) | copy-start | bytes 24580
  1.5 0.7 %copy-start.1 = (bf16[128,32]{0,1:T(8,128)(2,1)S(1)}, bf16[128,32]{0,1:T(8,128)(2,1)}, u32[]{:S(2)}) copy-start(bf16[128,32]{0,1:T(8,128)(2,1)} %param.33) | copy-start | bytes 24580

commit v2 on v1

v2 whole, which is shorter than its diff:
```python
import jax
import jax.numpy as jnp
from jax import lax
from jax.experimental import pallas as pl
from jax.experimental.pallas import tpu as pltpu
from jax.sharding import PartitionSpec as P

HEAD_DIM = 64
WINDOW = 64
ROWS = 256
TOKENS = 4096
EPS = 1e-6
COPIES = 120
MESH = pl.DeviceIdType.MESH
F32 = jnp.float32
BF16 = jnp.bfloat16
LINK = F32
NN = (((1,), (0,)), ((), ()))
NT = (((1,), (1,)), ((), ()))


def mm(a, b, dims=NN):
    return lax.dot_general(a, b, dims, preferred_element_type=F32)


def split(a):
    hi = a.astype(BF16)
    return hi, (a - hi.astype(F32)).astype(BF16)


def left(a):
    hi, lo = split(a)
    return jnp.concatenate([hi, lo], axis=1)


def right(b):
    hi, lo = split(b)
    return jnp.concatenate(
        [jnp.concatenate([hi, lo], axis=1), jnp.concatenate([hi, jnp.zeros_like(lo)], axis=1)], axis=0
    )


def dot3(a, b):
    both = mm(left(a), right(b))
    return both[:, 0:128] + both[:, 128:256]


def dot3_deep(a, b):
    ah, al = split(a)
    bh, bl = split(b)
    return mm(jnp.concatenate([ah, ah, al], axis=1), jnp.concatenate([bh, bl, bh], axis=0))


def silu(v):
    return v * jax.nn.sigmoid(v)


def layer_kernel(
    tokens, gain, aq, ak, av, dq, dk, dv, dz, bw, gw, ogain, ao, do, sink, shift, dlog,
    out,
    tok, normed, stage, w1, w2, kv, mats, rowmats, hsend, hall, pbuf, prec, send_sem, recv_sem, own_sem,
):
    sp = lax.axis_index("sp")
    x = lax.axis_index("tp")
    c = lax.rem(sp, 2)
    b = lax.div(sp, 2)
    z = lax.div(b, 4)
    y = lax.rem(b, 4)
    o = 1 - c

    open_scopes = []

    def phase(name):
        while open_scopes:
            open_scopes.pop().__exit__(None, None, None)
        if name:
            open_scopes.append(jax.named_scope(name))
            open_scopes[0].__enter__()

    def m4(v):
        return lax.rem(v + 4, 4)

    def dev(zz, yy, cc, xx):
        return {"sp": (zz * 4 + yy) * 2 + cc, "tp": xx}

    def dev_x(d):
        return dev(z, y, c, m4(x + d))

    def dev_y(d):
        return dev(z, m4(y + d), c, x)

    def dev_z(d):
        return dev(m4(z + d), y, c, x)

    def dev_b(d):
        bb = lax.rem(b + d + 16, 16)
        return {"sp": bb * 2 + c, "tp": x}

    partner = dev(z, y, o, x)
    sent = []

    def send(src, dst, device, landed):
        i = len(sent)
        copy = pltpu.make_async_remote_copy(
            src_ref=src, dst_ref=dst, send_sem=send_sem.at[i], recv_sem=recv_sem.at[i],
            device_id=device, device_id_type=MESH,
        )
        copy.start()
        sent.append(copy)
        return pltpu.make_async_remote_copy(
            src_ref=landed, dst_ref=landed, send_sem=send_sem.at[i], recv_sem=recv_sem.at[i],
            device_id=device, device_id_type=MESH,
        )

    phase("pack")
    attn_t, delta_t = ao[...], do[...]
    blank = jnp.zeros((60, 32), F32)
    for cc in range(2):
        cols = slice(64 * cc, 64 * cc + 64)
        small = jnp.concatenate([bw[cc].astype(F32), gw[cc].astype(F32), blank], axis=0).T.astype(BF16)
        stage[cc] = jnp.concatenate(
            [aq[:, cols], dq[:, cols], dk[:, cols], dv[:, cols], dz[:, cols], small, ak[...], av[...],
             attn_t[:, cols], delta_t[:, cols]],
            axis=1,
        )
    w1[z, y, c] = stage[c, :, 0:512]

    phase("barrier")
    barrier = pltpu.get_barrier_semaphore()
    peers = [partner]
    for d in (1, 2, 3):
        peers += [dev_x(d), dev_y(d), dev_z(d)]
    peers += [dev_b(1), dev_b(-1)]
    for peer in peers:
        pl.semaphore_signal(barrier, inc=1, device_id=peer, device_id_type=MESH)
    pl.semaphore_wait(barrier, len(peers))

    class Ring:
        def __init__(self, w, s, y_first):
            self.w, self.s, self.y_first = w, s, y_first
            self.waits = {}

        def slot(self, first, second, half=None):
            zz, yy = (z + second, y + first) if self.y_first else (z + first, y + second)
            ref = self.w.at[m4(zz), m4(yy), self.s]
            return ref if half is None else ref.at[pl.ds(16 * half, 16)]

        def dev1(self, d):
            return dev_y(d) if self.y_first else dev_z(d)

        def dev2(self, d):
            return dev_z(d) if self.y_first else dev_y(d)

        def across(self, f):
            for d in (1, -1):
                block = self.slot(f, 0)
                self.waits[f, d] = send(block, block, self.dev2(d), self.slot(f, -d))

        def relay(self, f):
            for d, half in ((1, 0), (-1, 1)):
                self.waits[f, d].wait_recv()
                block = self.slot(f, -d, half)
                self.waits[f, 2 * d] = send(block, block, self.dev2(d), self.slot(f, -2 * d, half))

        def begin(self):
            block = self.slot(0, 0)
            for d in (1, -1):
                self.waits[d] = send(block, block, self.dev1(d), self.slot(-d, 0))

        def near(self):
            for d, half in ((1, 0), (-1, 1)):
                self.waits[d].wait_recv()
                block = self.slot(-d, 0, half)
                self.waits[2 * d] = send(block, block, self.dev1(d), self.slot(-2 * d, 0, half))
            self.across(-1)
            self.across(1)

        def far(self):
            self.waits[2].wait_recv()
            self.waits[-2].wait_recv()
            self.across(2)

        def finish(self):
            for f in (0, -1, 1, 2):
                self.waits[f, 2].wait_recv()
                self.waits[f, -2].wait_recv()

    half_rows = pl.ds(128 * c, 128)
    other_rows = pl.ds(128 * o, 128)
    in_cols = pl.ds(0, 512)
    out_cols = pl.ds(512, 128)
    x_cols = pl.ds(pl.multiple_of(128 * x, 128), 128)

    def x_cols_of(d):
        return pl.ds(pl.multiple_of(128 * m4(x + d), 128), 128)

    phase("start")
    first = Ring(w1, c, True)
    second = Ring(w1, o, False)
    out_first = Ring(w2, c, True)
    out_second = Ring(w2, o, False)
    w_swap = send(stage.at[o, :, in_cols], w1.at[z, y, c], partner, w1.at[z, y, o])
    first.begin()
    tok_in = [send(tokens, tok.at[x, half_rows], dev_x(d), tok.at[m4(x - d), half_rows]) for d in (1, 3, 2)]
    tok_swap = [send(tokens, tok.at[x, half_rows], partner, tok.at[x, other_rows])]
    w2_swap = send(stage.at[o, :, out_cols], w2.at[z, y, c, :, x_cols], partner, w2.at[z, y, o, :, x_cols])
    first.across(0)
    own_tok = pltpu.make_async_copy(tokens, tok.at[x, half_rows], own_sem.at[0])
    own_tok.start()
    own_w2 = pltpu.make_async_copy(stage.at[c, :, out_cols], w2.at[z, y, c, :, x_cols], own_sem.at[1])
    own_w2.start()
    phase("swap")
    w_swap.wait_recv()
    second.begin()
    second.across(0)
    own_w2.wait()
    w2_swap.wait_recv()
    w2_in = [
        send(w2.at[z, y, :, :, x_cols], w2.at[z, y, :, :, x_cols], dev_x(d), w2.at[z, y, :, :, x_cols_of(-d)])
        for d in (1, 3, 2)
    ]
    phase("near")
    first.near()
    second.near()
    phase("tokens")
    for d, arrived in zip((1, 3, 2), tok_in):
        arrived.wait_recv()
        src = m4(x - d)
        tok_swap.append(send(tok.at[src, half_rows], tok.at[src, half_rows], partner, tok.at[src, other_rows]))
    phase("relay0")
    first.relay(0)
    second.relay(0)
    phase("far")
    first.far()
    second.far()
    phase("tokswap")
    own_tok.wait()
    for arrived in tok_swap:
        arrived.wait_recv()

    phase("norm")
    squares = jnp.zeros((ROWS, 1), F32)
    for k in range(4):
        wide = tok[k].astype(F32)
        squares = squares + jnp.sum(wide * wide, axis=-1, keepdims=True)
    inv = lax.rsqrt(squares * (1.0 / 1024.0) + EPS)
    for k in range(4):
        normed[k] = (tok[k].astype(F32) * inv * gain[:, 256 * k : 256 * k + 256]).astype(BF16)

    phase("relay1")
    for f in (-1, 1):
        first.relay(f)
        second.relay(f)
    phase("relay2")
    first.relay(2)
    second.relay(2)
    for arrived in w2_in:
        arrived.wait_recv()
    for ring in (out_first, out_second):
        ring.begin()
        ring.across(0)
    phase("wfinish")
    first.finish()
    second.finish()

    phase("proj")
    proj = mm(normed[0], w1[0].reshape(256, 512))
    for k in range(1, 4):
        proj = proj + mm(normed[k], w1[k].reshape(256, 512))
    t0, t1, t2 = proj[:, 0:128], proj[:, 128:256], proj[:, 256:384]
    kv[64:320, :] = proj[:, 384:512].astype(BF16)
    halo = [
        send(kv.at[pl.ds(256, 64)], kv.at[pl.ds(0, 64)], dev_b(1), kv.at[pl.ds(0, 64)]),
        send(kv.at[pl.ds(64, 64)], kv.at[pl.ds(320, 64)], dev_b(-1), kv.at[pl.ds(320, 64)]),
    ]
    att_q = t0[:, 0:64].astype(BF16)
    act_q = silu(t0[:, 64:128].astype(BF16).astype(F32))
    act_kv = silu(t1.astype(BF16).astype(F32))
    act_k, val = act_kv[:, 0:64], act_kv[:, 64:128]
    q = act_q * lax.rsqrt(jnp.sum(act_q * act_q, axis=-1, keepdims=True) + EPS) * HEAD_DIM**-0.5
    key = act_k * lax.rsqrt(jnp.sum(act_k * act_k, axis=-1, keepdims=True) + EPS)
    gate = silu(t2[:, 0:64].astype(BF16).astype(F32))

    phase("gates")
    lane = lax.broadcasted_iota(jnp.int32, (1, 128), 1)
    bias = jnp.where(lane == 64, shift[0, c], jnp.where(lane == 65, shift[1, c], 0.0))
    rate = jnp.exp(jnp.where(lane == 66, dlog[0, c], jnp.where(lane == 67, dlog[1, c], 0.0)))
    strength = jax.nn.sigmoid(t2 + bias)
    softplus = jnp.maximum(t2, 0.0) + jnp.log1p(jnp.exp(-jnp.abs(t2)))
    decay = jnp.where((lane == 66) | (lane == 67), -rate * softplus * (1.0 / TOKENS), 0.0)

    row = lax.broadcasted_iota(jnp.int32, (128, 128), 0)
    col = lax.broadcasted_iota(jnp.int32, (128, 128), 1)
    masks = (row >= col, row <= col)
    unit = jnp.where(row == col, 1.0, 0.0)
    near16 = lax.shift_right_logical(row, 4) == lax.shift_right_logical(col, 4)

    g_hi = decay.astype(BF16)
    rest = decay - g_hi.astype(F32)
    g_mid = rest.astype(BF16)
    g_lo = (rest - g_mid.astype(F32)).astype(BF16)
    g_parts = jnp.concatenate(
        [part[128 * h : 128 * h + 128, 64:128] for h in range(2) for part in (g_hi, g_mid, g_lo)], axis=1
    )
    sums = [mm(jnp.where(mask, 1.0, 0.0).astype(BF16), g_parts) for mask in masks]
    sub = lax.broadcasted_iota(jnp.int32, (1, 192), 1)
    picked = jnp.where((sub & 63) == 2, sums[0][:, 0:192], sums[1][:, 0:192])
    picked2 = jnp.where((sub & 63) == 2, sums[0][:, 192:384], sums[1][:, 192:384])
    g_all = jnp.concatenate([p[:, 0:64] + p[:, 64:128] + p[:, 128:192] for p in (picked, picked2)], axis=0)
    turned = jnp.concatenate([key, g_all], axis=1).T
    key_t = turned[0:64]
    key_h, key_l = split(key)
    q_h, q_l = split(q)
    kt_h, kt_l = split(key_t)
    q3 = jnp.concatenate([q_h, q_h, q_l], axis=1)
    key3 = jnp.concatenate([key_h, key_h, key_l], axis=1)
    kt3 = jnp.concatenate([kt_h, kt_l, kt_h], axis=0)

    phase("rings1")
    out_first.near()
    out_second.near()

    phase("delta1")
    lane2 = lax.broadcasted_iota(jnp.int32, (64, 128), 1)
    row2 = lax.broadcasted_iota(jnp.int32, (64, 128), 0)
    eye2 = jnp.where(lane2 == row2 + 64, 1.0, 0.0)
    chains = [(way, h) for way in range(2) for h in range(2)]
    low, scores_d, sides, grown, key_end, end, d = {}, {}, {}, {}, {}, {}, {}
    for h in range(2):
        hs = slice(128 * h, 128 * h + 128)
        pairs = mm(jnp.concatenate([q3[hs], key3[hs]], axis=0), kt3[:, hs])
        for way in range(2):
            at = way, h
            beta = strength[hs, 64 + way : 65 + way]
            g_col = g_all[hs, 2 + way : 3 + way]
            g_row = turned[66 + way : 67 + way, hs]
            g_end = g_col[127:128] if way == 0 else g_col[0:1]
            decays = jnp.exp(jnp.where(masks[way], g_col - g_row, -jnp.inf))
            low[at] = jnp.where(row == col, 0.0, beta * pairs[128:256] * decays)
            scores_d[at] = pairs[0:128] * decays
            up = jnp.exp(g_col)
            grown[at] = up * q[hs]
            sides[at] = jnp.concatenate([beta * val[hs], (beta * up) * key[hs]], axis=1)
            key_end[at] = key_t[:, hs] * jnp.exp(g_end - g_row)
            end[at] = jnp.exp(g_end)
    d1 = {at: jnp.where(near16, low[at], 0.0) for at in chains}
    off = {at: jnp.where(near16, 0.0, low[at]) for at in chains}
    d2 = {at: dot3(d1[at], d1[at]) for at in chains}
    inner = {at: unit - d1[at] for at in chains}
    d4 = {at: dot3(d2[at], d2[at]) for at in chains}
    inner = {at: inner[at] + dot3(inner[at], d2[at]) for at in chains}
    d8 = {at: dot3(d4[at], d4[at]) for at in chains}
    inner = {at: inner[at] + dot3(inner[at], d4[at]) for at in chains}
    inner = {at: inner[at] + dot3(inner[at], d8[at]) for at in chains}
    phase("rings2")
    out_first.relay(0)
    out_second.relay(0)
    out_first.far()
    out_second.far()
    phase("delta2")
    m1 = {at: dot3(inner[at], off[at]) for at in chains}
    uw = {at: dot3(inner[at], sides[at]) for at in chains}
    m2 = {at: dot3(m1[at], m1[at]) for at in chains}
    uw = {at: uw[at] - dot3(m1[at], uw[at]) for at in chains}
    m4_ = {at: dot3(m2[at], m2[at]) for at in chains}
    uw = {at: uw[at] + dot3(m2[at], uw[at]) for at in chains}
    uw = {at: uw[at] + dot3(m4_[at], uw[at]) for at in chains}
    phase("rings3")
    for f in (-1, 1, 2):
        out_first.relay(f)
        out_second.relay(f)
    phase("final")

    def after(later, earlier):
        return dot3_deep(later[:, 64:128], earlier) + jnp.where(lane2 < 64, later, 0.0)

    maps = {}
    for at in chains:
        final = dot3(key_end[at], uw[at])
        maps[at] = jnp.where(lane2 < 64, final, end[at] * eye2 - final)
    for way in range(2):
        block_map = after(maps[way, 1 - way], maps[way, way])
        mats[y, way] = (block_map - eye2).astype(LINK)
    phase("scan1send")
    scan1 = [send(mats.at[y], mats.at[y], dev_y(d), mats.at[m4(y - d)]) for d in (1, 3, 2)]

    phase("reads")
    local, reads = {}, {}
    for way, h in chains:
        at = way, h
        read = dot3(scores_d[at], uw[at])
        local[at] = read[:, 0:64]
        reads[at] = grown[at] - read[:, 64:128]
        if h != way:
            passed = dot3_deep(reads[at], maps[way, way])
            local[at] = local[at] + passed[:, 0:64]
            reads[at] = passed[:, 64:128]
    local_sum = jnp.concatenate([local[0, h] + local[1, h] for h in range(2)], axis=0)
    reads_all = jnp.concatenate(
        [jnp.concatenate([reads[0, h], reads[1, h]], axis=1) for h in range(2)], axis=0
    )

    phase("halo")
    for arrived in halo:
        arrived.wait_recv()
    phase("attn")
    scores = mm(att_q, kv[:, 0:64], NT) * HEAD_DIM**-0.5
    q_pos = lax.broadcasted_iota(jnp.int32, (ROWS, ROWS + 2 * WINDOW), 0)
    k_pos = lax.broadcasted_iota(jnp.int32, (ROWS, ROWS + 2 * WINDOW), 1) - WINDOW
    seen = k_pos + b * ROWS
    allowed = (jnp.abs(q_pos - k_pos) <= WINDOW) & (seen >= 0) & (seen < TOKENS)
    scores = jnp.where(allowed, scores, -jnp.inf)
    top = jnp.maximum(jnp.max(scores, axis=-1, keepdims=True), sink[c])
    weights = jnp.exp(scores - top)
    total = jnp.sum(weights, axis=-1, keepdims=True) + jnp.exp(sink[c] - top)
    weights = (weights / total).astype(BF16)
    attn_heads = mm(weights, kv[:, 64:128])

    phase("scan1wait")
    for arrived in scan1:
        arrived.wait_recv()

    phase("compose")
    entry = []
    for way in range(2):
        m = [mats[k if way == 0 else 3 - k, way].astype(F32) + eye2 for k in range(4)]
        place = y if way == 0 else 3 - y
        two = after(m[1], m[0])
        three = after(m[2], two)
        rowmats[z, way] = (after(after(m[3], m[2]), two) - eye2).astype(LINK)
        entry.append(
            jnp.where(place == 0, eye2, jnp.where(place == 1, m[0], jnp.where(place == 2, two, three)))
        )
    phase("scan2send")
    scan2 = [send(rowmats.at[z], rowmats.at[z], dev_z(d), rowmats.at[m4(z - d)]) for d in (1, 3, 2)]
    phase("scan2wait")
    for arrived in scan2:
        arrived.wait_recv()
    phase("states")
    states = []
    for way in range(2):
        m = [rowmats[k if way == 0 else 3 - k, way].astype(F32) + eye2 for k in range(3)]
        place = z if way == 0 else 3 - z
        s1 = m[0][:, 0:64]
        s2 = dot3_deep(m[1][:, 64:128], s1) + m[1][:, 0:64]
        s3 = dot3_deep(m[2][:, 64:128], s2) + m[2][:, 0:64]
        s = jnp.where(place == 0, 0.0, jnp.where(place == 1, s1, jnp.where(place == 2, s2, s3)))
        states.append(dot3_deep(entry[way][:, 64:128], s) + entry[way][:, 0:64])

    reads_h, reads_l = split(reads_all)
    states_h, states_l = split(jnp.concatenate(states, axis=0))
    whole = mm(
        jnp.concatenate([reads_h, reads_l], axis=1),
        jnp.concatenate([states_h, states_h], axis=0),
    )
    whole = local_sum + whole + mm(reads_h, states_l)
    scaled = whole * lax.rsqrt(jnp.mean(whole * whole, axis=-1, keepdims=True) + EPS) * ogain[...]
    heads = jnp.concatenate([attn_heads, scaled * gate], axis=1).astype(BF16)
    for k in range(4):
        hsend[k, 0:32] = heads[32 * k : 32 * k + 32]
        hsend[k, 32:64] = heads[128 + 32 * k : 160 + 32 * k]
    phase("headsend")
    head_in = [send(hsend.at[m4(x + d)], hall.at[x], dev_x(d), hall.at[m4(x - d)]) for d in (1, 3, 2)]
    hall[x] = hsend[x]
    phase("w2finish")
    out_first.finish()
    out_second.finish()
    phase("headwait")
    for arrived in head_in:
        arrived.wait_recv()
    phase("outmm")
    gathered = jnp.concatenate([hall[k] for k in range(4)], axis=1)
    for k in range(4):
        part = mm(gathered, w2[k].reshape(256, 512), NT)
        pbuf[0, :, 256 * k : 256 * k + 256] = part[0:32]
        pbuf[1, :, 256 * k : 256 * k + 256] = part[32:64]
    phase("last")
    last = send(pbuf.at[o], prec, partner, prec)
    last.wait_recv()
    out[...] = pbuf[c] + prec[...]
    phase("drain")
    for copy in sent:
        copy.wait_send()
    phase(None)


def per_device(
    tokens, norm_gain, attn_query, attn_key, attn_value, sink_logit, delta_query, delta_key, delta_value,
    delta_gate, beta_weight, decay_weight, beta_shift, decay_log, out_gain, attn_out, delta_out,
):
    vmem = pl.BlockSpec(memory_space=pltpu.VMEM)
    smem = pl.BlockSpec(memory_space=pltpu.SMEM)
    summed = pl.pallas_call(
        layer_kernel,
        out_shape=jax.ShapeDtypeStruct((32, 1024), F32),
        in_specs=[vmem] * 14 + [smem] * 3,
        out_specs=vmem,
        scratch_shapes=[
            pltpu.VMEM((4, 256, 256), BF16),
            pltpu.VMEM((4, 256, 256), BF16),
            pltpu.VMEM((2, 32, 640), BF16),
            pltpu.VMEM((4, 4, 2, 32, 512), BF16),
            pltpu.VMEM((4, 4, 2, 32, 512), BF16),
            pltpu.VMEM((384, 128), BF16),
            pltpu.VMEM((4, 2, 64, 128), LINK),
            pltpu.VMEM((4, 2, 64, 128), LINK),
            pltpu.VMEM((4, 64, 128), BF16),
            pltpu.VMEM((4, 64, 128), BF16),
            pltpu.VMEM((2, 32, 1024), F32),
            pltpu.VMEM((32, 1024), F32),
            pltpu.SemaphoreType.DMA((COPIES,)),
            pltpu.SemaphoreType.DMA((COPIES,)),
            pltpu.SemaphoreType.DMA((2,)),
        ],
        compiler_params=pltpu.CompilerParams(collective_id=0, has_side_effects=True, vmem_limit_bytes=24 * 2**20),
    )(
        tokens, norm_gain.reshape(1, -1), attn_query, attn_key, attn_value, delta_query, delta_key, delta_value,
        delta_gate, beta_weight.transpose(1, 2, 0), decay_weight.transpose(1, 2, 0), out_gain.reshape(1, -1),
        attn_out.T, delta_out.T, sink_logit, beta_shift, decay_log,
    )
    return summed.astype(BF16)


def solution(mesh):
    return jax.shard_map(
        per_device,
        mesh=mesh,
        in_specs=(
            P("sp", "tp"), P(), P("sp", "tp"), P("sp", "tp"), P("sp", "tp"), P("tp"), P("sp", "tp"),
            P("sp", "tp"), P("sp", "tp"), P("sp", "tp"), P("sp", "tp", None), P("sp", "tp", None),
            P(None, "tp"), P(None, "tp"), P(), P("tp", "sp"), P("tp", "sp"),
        ),
        out_specs=P(("sp", "tp"), None),
        check_vma=False,
    )
```

time: 60.3 us -> 64.8 us (1.075)
  local copies, waits for them, and re-layouts: 4.41 us -> 9.8 us
  Pallas kernels: 55.6 us -> 53.6 us
    unnamed x11 -> x34, local copies, waits for them, and re-layouts: 3.7 us -> 9.8 us
    pallas_call x1, Pallas kernels: 55.6 us -> 53.6 us  [per_device(): pl.pallas_call(layer_kernel, out_shape=jax.ShapeDtypeStruct((32, 1024), F...]
where the time goes in v2:
time: 64.8 us; the launch traced here: 64.1 us
  Pallas kernels  53.6 us (83%)
  local copies, waits for them, and re-layouts  9.8 us (15%)
    pallas_call x1, Pallas kernels, per_device(): pl.pallas_call(layer_kernel, out_shape=jax.ShapeDtypeStruct((32, 1024), F...  53.6 us
    unnamed x34, local copies, waits for them, and re-layouts  9.8 us

profile of v2, /device:TPU:1, one launch (start us, length us, event | category | flops | bytes accessed | tf_op | source)
XLA Modules:
  0.0 64.1 jit_solution(10104037941525235909)
XLA Ops:
  0.0 0.0 copy-start.1
  0.0 0.0 copy-start.12
  0.0 0.0 copy-start.13
  0.0 0.0 copy-start.11
  0.0 0.7 %copy-done.1 = bf16[32,128]{1,0:T(8,128)(2,1)S(1)} copy-done((bf16[32,128]{1,0:T(8,128)(2,1)S(1)}, bf16[32,128]{1,0:T(8,128)(2,1)}, u32[]{:S(2)}) %copy-start.1) | copy-done | bytes 8216
  0.7 0.0 copy-done.12
  0.7 0.0 copy-done.13
  0.7 0.0 copy-done.11
  0.7 0.0 copy-start
  0.7 0.8 %copy-done = bf16[128,256]{1,0:T(8,128)(2,1)S(1)} copy-done((bf16[128,256]{1,0:T(8,128)(2,1)S(1)}, bf16[128,256]{1,0:T(8,128)(2,1)}, u32[]{:S(2)}) %copy-start) | copy-done | bytes 65560
  1.6 0.0 copy-start.2
  1.6 0.7 %copy-done.2 = bf16[32,64]{1,0:T(8,128)(2,1)S(1)} copy-done((bf16[32,64]{1,0:T(8,128)(2,1)S(1)}, bf16[32,64]{1,0:T(8,128)(2,1)}, u32[]{:S(2)}) %copy-start.2) | copy-done | bytes 4120
  2.3 0.0 copy-start.3
  2.3 0.7 %copy-done.3 = bf16[32,64]{1,0:T(8,128)(2,1)S(1)} copy-done((bf16[32,64]{1,0:T(8,128)(2,1)S(1)}, bf16[32,64]{1,0:T(8,128)(2,1)}, u32[]{:S(2)}) %copy-start.3) | copy-done | bytes 4120
  3.0 0.0 copy-start.4
  3.0 0.7 %copy-done.4 = bf16[32,128]{1,0:T(8,128)(2,1)S(1)} copy-done((bf16[32,128]{1,0:T(8,128)(2,1)S(1)}, bf16[32,128]{1,0:T(8,128)(2,1)}, u32[]{:S(2)}) %copy-start.4) | copy-done | bytes 8216
  3.7 0.0 copy-start.5
  3.7 0.7 %copy-done.5 = bf16[32,128]{1,0:T(8,128)(2,1)S(1)} copy-done((bf16[32,128]{1,0:T(8,128)(2,1)S(1)}, bf16[32,128]{1,0:T(8,128)(2,1)}, u32[]{:S(2)}) %copy-start.5) | copy-done | bytes 8216
  4.4 0.0 copy-start.6
  4.4 0.7 %copy-done.6 = bf16[32,128]{1,0:T(8,128)(2,1)S(1)} copy-done((bf16[32,128]{1,0:T(8,128)(2,1)S(1)}, bf16[32,128]{1,0:T(8,128)(2,1)}, u32[]{:S(2)}) %copy-start.6) | copy-done | bytes 8216
  5.1 0.0 copy-start.7
  5.1 0.7 %copy-done.7 = bf16[32,128]{1,0:T(8,128)(2,1)S(1)} copy-done((bf16[32,128]{1,0:T(8,128)(2,1)S(1)}, bf16[32,128]{1,0:T(8,128)(2,1)}, u32[]{:S(2)}) %copy-start.7) | copy-done | bytes 8216
  5.8 0.0 copy-start.8
  5.8 0.7 %copy-done.8 = bf16[128,32]{0,1:T(8,128)(2,1)S(1)} copy-done((bf16[128,32]{0,1:T(8,128)(2,1)S(1)}, bf16[128,32]{0,1:T(8,128)(2,1)}, u32[]{:S(2)}) %copy-start.8) | copy-done | bytes 8216
  6.4 0.0 copy-start.9
  6.5 0.7 %copy-done.9 = bf16[128,32]{0,1:T(8,128)(2,1)S(1)} copy-done((bf16[128,32]{0,1:T(8,128)(2,1)S(1)}, bf16[128,32]{0,1:T(8,128)(2,1)}, u32[]{:S(2)}) %copy-start.9) | copy-done | bytes 8216
  7.1 0.0 copy-start.10
  7.1 0.7 %copy-done.10 = f32[1024]{0:T(1024)S(1)} copy-done((f32[1024]{0:T(1024)S(1)}, f32[1024]{0:T(1024)}, u32[]{:S(2)}) %copy-start.10) | copy-done | bytes 4120
  7.8 0.0 copy-start.14
  7.8 0.7 %copy-done.14 = f32[2,2]{1,0:T(2,128)S(1)} copy-done((f32[2,2]{1,0:T(2,128)S(1)}, f32[2,2]{1,0:T(2,128)}, u32[]{:S(2)}) %copy-start.14) | copy-done | bytes 40
  8.5 0.0 copy-start.15
  8.5 0.7 %copy-done.15 = f32[64]{0:T(128)S(1)} copy-done((f32[64]{0:T(128)S(1)}, f32[64]{0:T(128)}, u32[]{:S(2)}) %copy-start.15) | copy-done | bytes 280
  9.2 0.0 copy-start.16
  9.2 0.7 %copy-done.16 = f32[2]{0:T(128)S(1)} copy-done((f32[2]{0:T(128)S(1)}, f32[2]{0:T(128)}, u32[]{:S(2)}) %copy-start.16) | copy-done | bytes 32
  9.8 53.6 %shard_map.163 = f32[32,1024]{1,0:T(8,128)S(1)} custom-call(bf16[128,256]{1,0:T(8,128)(2,1)S(1)} %copy-done, f32[1,1024]{1,0:T(1,128)S(1)} %bitcast.8, bf16[32,128]{1,0:T(8,128)(2,1)S(1)} %copy-done.1, bf16[32,64]{1,0:T(8,128)(2,1)S(1)} %copy-done.2, bf16[32,64]{1,0:T(8,128)(2,1)S(1)} %copy-done.3, bf16[32,128]{1,0:T(8,128)(2,1)S(1)} %copy-done.4, ...), custom_call_target="tpu_custom_call" | custom-call | tf_op jit(solution)/shard_map/pallas_call | solution.py:493
  63.4 0.6 convert_element_type.3
Async XLA Ops:
  0.0 0.7 %copy-start.1 = (bf16[32,128]{1,0:T(8,128)(2,1)S(1)}, bf16[32,128]{1,0:T(8,128)(2,1)}, u32[]{:S(2)}) copy-start(bf16[32,128]{1,0:T(8,128)(2,1)} %aq.1) | copy-start | bytes 24580
  0.0 0.7 %copy-start.12 = (bf16[32,2,2]{0,2,1:T(2,128)(2,1)S(1)}, bf16[32,2,2]{0,2,1:T(2,128)(2,1)}, u32[]{:S(2)}) copy-start(bf16[32,2,2]{0,2,1:T(2,128)(2,1)} %param.28) | copy-start | bytes 772
  0.0 0.7 %copy-start.13 = (f32[2,2]{1,0:T(2,128)S(1)}, f32[2,2]{1,0:T(2,128)}, u32[]{:S(2)}) copy-start(f32[2,2]{1,0:T(2,128)} %shift.1) | copy-start | bytes 52
  0.0 0.7 %copy-start.11 = (bf16[32,2,2]{0,2,1:T(2,128)(2,1)S(1)}, bf16[32,2,2]{0,2,1:T(2,128)(2,1)}, u32[]{:S(2)}) copy-start(bf16[32,2,2]{0,2,1:T(2,128)(2,1)} %param.27) | copy-start | bytes 772
  0.7 0.8 %copy-start = (bf16[128,256]{1,0:T(8,128)(2,1)S(1)}, bf16[128,256]{1,0:T(8,128)(2,1)}, u32[]{:S(2)}) copy-start(bf16[128,256]{1,0:T(8,128)(2,1)} %tokens.1) | copy-start | bytes 196612
  1.6 0.7 %copy-start.2 = (bf16[32,64]{1,0:T(8,128)(2,1)S(1)}, bf16[32,64]{1,0:T(8,128)(2,1)}, u32[]{:S(2)}) copy-start(bf16[32,64]{1,0:T(8,128)(2,1)} %ak.1) | copy-start | bytes 12292
  2.3 0.7 %copy-start.3 = (bf16[32,64]{1,0:T(8,128)(2,1)S(1)}, bf16[32,64]{1,0:T(8,128)(2,1)}, u32[]{:S(2)}) copy-start(bf16[32,64]{1,0:T(8,128)(2,1)} %av.1) | copy-start | bytes 12292
  3.0 0.7 %copy-start.4 = (bf16[32,128]{1,0:T(8,128)(2,1)S(1)}, bf16[32,128]{1,0:T(8,128)(2,1)}, u32[]{:S(2)}) copy-start(bf16[32,128]{1,0:T(8,128)(2,1)} %dq.1) | copy-start | bytes 24580
  3.7 0.7 %copy-start.5 = (bf16[32,128]{1,0:T(8,128)(2,1)S(1)}, bf16[32,128]{1,0:T(8,128)(2,1)}, u32[]{:S(2)}) copy-start(bf16[32,128]{1,0:T(8,128)(2,1)} %dk.1) | copy-start | bytes 24580
  4.4 0.7 %copy-start.6 = (bf16[32,128]{1,0:T(8,128)(2,1)S(1)}, bf16[32,128]{1,0:T(8,128)(2,1)}, u32[]{:S(2)}) copy-start(bf16[32,128]{1,0:T(8,128)(2,1)} %dv.1) | copy-start | bytes 24580
  5.1 0.7 %copy-start.7 = (bf16[32,128]{1,0:T(8,128)(2,1)S(1)}, bf16[32,128]{1,0:T(8,128)(2,1)}, u32[]{:S(2)}) copy-start(bf16[32,128]{1,0:T(8,128)(2,1)} %dz.1) | copy-start | bytes 24580
  5.8 0.7 %copy-start.8 = (bf16[128,32]{0,1:T(8,128)(2,1)S(1)}, bf16[128,32]{0,1:T(8,128)(2,1)}, u32[]{:S(2)}) copy-start(bf16[128,32]{0,1:T(8,128)(2,1)} %param.32) | copy-start | bytes 24580
  6.4 0.7 %copy-start.9 = (bf16[128,32]{0,1:T(8,128)(2,1)S(1)}, bf16[128,32]{0,1:T(8,128)(2,1)}, u32[]{:S(2)}) copy-start(bf16[128,32]{0,1:T(8,128)(2,1)} %param.33) | copy-start | bytes 24580
  7.1 0.7 %copy-start.10 = (f32[1024]{0:T(1024)S(1)}, f32[1024]{0:T(1024)}, u32[]{:S(2)}) copy-start(f32[1024]{0:T(1024)} %param.18) | copy-start | bytes 12292
  7.8 0.7 %copy-start.14 = (f32[2,2]{1,0:T(2,128)S(1)}, f32[2,2]{1,0:T(2,128)}, u32[]{:S(2)}) copy-start(f32[2,2]{1,0:T(2,128)} %dlog.1) | copy-start | bytes 52
  8.5 0.7 %copy-start.15 = (f32[64]{0:T(128)S(1)}, f32[64]{0:T(128)}, u32[]{:S(2)}) copy-start(f32[64]{0:T(128)} %param.31) | copy-start | bytes 772
  9.2 0.7 %copy-start.16 = (f32[2]{0:T(128)S(1)}, f32[2]{0:T(128)}, u32[]{:S(2)}) copy-start(f32[2]{0:T(128)} %sink.1) | copy-start | bytes 28

commit v3 on v2

--- a/solution.py
+++ b/solution.py
@@ -56,8 +56,10 @@
 
 
 def layer_kernel(
-    tokens, gain, aq, ak, av, dq, dk, dv, dz, bw, gw, ogain, ao, do, sink, shift, dlog,
+    tokens_in, gain_in, aq_in, ak_in, av_in, dq_in, dk_in, dv_in, dz_in, bw_in, gw_in, ogain_in, ao_in, do_in,
+    sink_in, shift_in, dlog_in,
     out,
+    gain, aq, ak, av, dq, dk, dv, dz, bw, gw, ogain, ao, do, sink, shift, dlog,
     tok, normed, stage, w1, w2, kv, mats, rowmats, hsend, hall, pbuf, prec, send_sem, recv_sem, own_sem,
 ):
     sp = lax.axis_index("sp")
@@ -86,11 +88,11 @@
     def dev_x(d):
         return dev(z, y, c, m4(x + d))
 
-    def dev_y(d):
-        return dev(z, m4(y + d), c, x)
-
-    def dev_z(d):
-        return dev(m4(z + d), y, c, x)
+    def dev_y(d, core=c):
+        return dev(z, m4(y + d), core, x)
+
+    def dev_z(d, core=c):
+        return dev(m4(z + d), y, core, x)
 
     def dev_b(d):
         bb = lax.rem(b + d + 16, 16)
@@ -112,6 +114,29 @@
             device_id=device, device_id_type=MESH,
         )
 
+    phase("load")
+    half_rows = pl.ds(128 * c, 128)
+    other_rows = pl.ds(128 * o, 128)
+    tokens = tok.at[x, half_rows]
+    loads = [
+        pltpu.make_async_copy(src, dst, own_sem.at[i])
+        for i, (src, dst) in enumerate(
+            [(aq_in, aq), (ak_in, ak), (av_in, av), (dq_in, dq), (dk_in, dk), (dv_in, dv), (dz_in, dz), (bw_in, bw),
+             (gw_in, gw), (ao_in, ao), (do_in, do), (tokens_in, tokens), (gain_in, gain), (ogain_in, ogain),
+             (sink_in, sink), (shift_in, shift), (dlog_in, dlog)]
+        )
+    ]
+    for load in loads:
+        load.start()
+    barrier = pltpu.get_barrier_semaphore()
+    peers = [partner]
+    for d in (1, 2, 3):
+        peers += [dev_x(d), dev_y(d), dev_z(d), dev_y(d, o), dev_z(d, o)]
+    peers += [dev_b(1), dev_b(-1)]
+    for peer in peers:
+        pl.semaphore_signal(barrier, inc=1, device_id=peer, device_id_type=MESH)
+    for load in loads[:11]:
+        load.wait()
     phase("pack")
     attn_t, delta_t = ao[...], do[...]
     blank = jnp.zeros((60, 32), F32)
@@ -126,18 +151,11 @@
     w1[z, y, c] = stage[c, :, 0:512]
 
     phase("barrier")
-    barrier = pltpu.get_barrier_semaphore()
-    peers = [partner]
-    for d in (1, 2, 3):
-        peers += [dev_x(d), dev_y(d), dev_z(d)]
-    peers += [dev_b(1), dev_b(-1)]
-    for peer in peers:
-        pl.semaphore_signal(barrier, inc=1, device_id=peer, device_id_type=MESH)
     pl.semaphore_wait(barrier, len(peers))
 
     class Ring:
-        def __init__(self, w, s, y_first):
-            self.w, self.s, self.y_first = w, s, y_first
+        def __init__(self, w, s, y_first, source=None):
+            self.w, self.s, self.y_first, self.source = w, s, y_first, source
             self.waits = {}
 
         def slot(self, first, second, half=None):
@@ -145,16 +163,22 @@
             ref = self.w.at[m4(zz), m4(yy), self.s]
             return ref if half is None else ref.at[pl.ds(16 * half, 16)]
 
-        def dev1(self, d):
-            return dev_y(d) if self.y_first else dev_z(d)
-
-        def dev2(self, d):
-            return dev_z(d) if self.y_first else dev_y(d)
+        def twin(self, _):
+            return self.w.at[z, y, 1 - self.s]
+
+        def dev1(self, d, core=c):
+            return dev_y(d, core) if self.y_first else dev_z(d, core)
+
+        def dev2(self, d, core=c):
+            return dev_z(d, core) if self.y_first else dev_y(d, core)
 
         def across(self, f):
             for d in (1, -1):
-                block = self.slot(f, 0)
-                self.waits[f, d] = send(block, block, self.dev2(d), self.slot(f, -d))
+                if f == 0 and self.source is not None:
+                    self.waits[f, d] = send(self.source, self.twin(0), self.dev2(d, o), self.slot(f, -d))
+                else:
+                    block = self.slot(f, 0)
+                    self.waits[f, d] = send(block, block, self.dev2(d), self.slot(f, -d))
 
         def relay(self, f):
             for d, half in ((1, 0), (-1, 1)):
@@ -165,7 +189,10 @@
         def begin(self):
             block = self.slot(0, 0)
             for d in (1, -1):
-                self.waits[d] = send(block, block, self.dev1(d), self.slot(-d, 0))
+                if self.source is not None:
+                    self.waits[d] = send(self.source, self.twin(0), self.dev1(d, o), self.slot(-d, 0))
+                else:
+                    self.waits[d] = send(block, block, self.dev1(d), self.slot(-d, 0))
 
         def near(self):
             for d, half in ((1, 0), (-1, 1)):
@@ -185,8 +212,6 @@
                 self.waits[f, 2].wait_recv()
                 self.waits[f, -2].wait_recv()
 
-    half_rows = pl.ds(128 * c, 128)
-    other_rows = pl.ds(128 * o, 128)
     in_cols = pl.ds(0, 512)
     out_cols = pl.ds(512, 128)
     x_cols = pl.ds(pl.multiple_of(128 * x, 128), 128)
@@ -196,23 +221,23 @@
 
     phase("start")
     first = Ring(w1, c, True)
-    second = Ring(w1, o, False)
+    second = Ring(w1, o, False, stage.at[o, :, in_cols])
     out_first = Ring(w2, c, True)
     out_second = Ring(w2, o, False)
+    first.begin()
+    second.begin()
+    first.across(0)
+    second.across(0)
+    for load in loads[11:]:
+        load.wait()
+    tok_in = [send(tokens, tokens, dev_x(d), tok.at[m4(x - d), half_rows]) for d in (1, 3, 2)]
     w_swap = send(stage.at[o, :, in_cols], w1.at[z, y, c], partner, w1.at[z, y, o])
-    first.begin()
-    tok_in = [send(tokens, tok.at[x, half_rows], dev_x(d), tok.at[m4(x - d), half_rows]) for d in (1, 3, 2)]
-    tok_swap = [send(tokens, tok.at[x, half_rows], partner, tok.at[x, other_rows])]
+    tok_swap = [send(tokens, tokens, partner, tok.at[x, other_rows])]
     w2_swap = send(stage.at[o, :, out_cols], w2.at[z, y, c, :, x_cols], partner, w2.at[z, y, o, :, x_cols])
-    first.across(0)
-    own_tok = pltpu.make_async_copy(tokens, tok.at[x, half_rows], own_sem.at[0])
-    own_tok.start()
-    own_w2 = pltpu.make_async_copy(stage.at[c, :, out_cols], w2.at[z, y, c, :, x_cols], own_sem.at[1])
+    own_w2 = pltpu.make_async_copy(stage.at[c, :, out_cols], w2.at[z, y, c, :, x_cols], own_sem.at[17])
     own_w2.start()
     phase("swap")
     w_swap.wait_recv()
-    second.begin()
-    second.across(0)
     own_w2.wait()
     w2_swap.wait_recv()
     w2_in = [
@@ -234,7 +259,6 @@
     first.far()
     second.far()
     phase("tokswap")
-    own_tok.wait()
     for arrived in tok_swap:
         arrived.wait_recv()
 
@@ -352,11 +376,6 @@
     d8 = {at: dot3(d4[at], d4[at]) for at in chains}
     inner = {at: inner[at] + dot3(inner[at], d4[at]) for at in chains}
     inner = {at: inner[at] + dot3(inner[at], d8[at]) for at in chains}
-    phase("rings2")
-    out_first.relay(0)
-    out_second.relay(0)
-    out_first.far()
-    out_second.far()
     phase("delta2")
     m1 = {at: dot3(inner[at], off[at]) for at in chains}
     uw = {at: dot3(inner[at], sides[at]) for at in chains}
@@ -365,10 +384,6 @@
     m4_ = {at: dot3(m2[at], m2[at]) for at in chains}
     uw = {at: uw[at] + dot3(m2[at], uw[at]) for at in chains}
     uw = {at: uw[at] + dot3(m4_[at], uw[at]) for at in chains}
-    phase("rings3")
-    for f in (-1, 1, 2):
-        out_first.relay(f)
-        out_second.relay(f)
     phase("final")
 
     def after(later, earlier):
@@ -384,6 +399,11 @@
     phase("scan1send")
     scan1 = [send(mats.at[y], mats.at[y], dev_y(d), mats.at[m4(y - d)]) for d in (1, 3, 2)]
 
+    phase("rings2")
+    out_first.relay(0)
+    out_second.relay(0)
+    out_first.far()
+    out_second.far()
     phase("reads")
     local, reads = {}, {}
     for way, h in chains:
@@ -433,6 +453,10 @@
         )
     phase("scan2send")
     scan2 = [send(rowmats.at[z], rowmats.at[z], dev_z(d), rowmats.at[m4(z - d)]) for d in (1, 3, 2)]
+    phase("rings3")
+    for f in (-1, 1, 2):
+        out_first.relay(f)
+        out_second.relay(f)
     phase("scan2wait")
     for arrived in scan2:
         arrived.wait_recv()
@@ -488,14 +512,35 @@
     tokens, norm_gain, attn_query, attn_key, attn_value, sink_logit, delta_query, delta_key, delta_value,
     delta_gate, beta_weight, decay_weight, beta_shift, decay_log, out_gain, attn_out, delta_out,
 ):
+    operands = (
+        tokens, norm_gain.reshape(1, -1), attn_query, attn_key, attn_value, delta_query, delta_key, delta_value,
+        delta_gate, beta_weight.transpose(1, 2, 0), decay_weight.transpose(1, 2, 0), out_gain.reshape(1, -1),
+        attn_out.T, delta_out.T, sink_logit, beta_shift, decay_log,
+    )
+    hbm = pl.BlockSpec(memory_space=pltpu.HBM)
     vmem = pl.BlockSpec(memory_space=pltpu.VMEM)
-    smem = pl.BlockSpec(memory_space=pltpu.SMEM)
     summed = pl.pallas_call(
         layer_kernel,
         out_shape=jax.ShapeDtypeStruct((32, 1024), F32),
-        in_specs=[vmem] * 14 + [smem] * 3,
+        in_specs=[hbm] * 17,
         out_specs=vmem,
         scratch_shapes=[
+            pltpu.VMEM((1, 1024), F32),
+            pltpu.VMEM((32, 128), BF16),
+            pltpu.VMEM((32, 64), BF16),
+            pltpu.VMEM((32, 64), BF16),
+            pltpu.VMEM((32, 128), BF16),
+            pltpu.VMEM((32, 128), BF16),
+            pltpu.VMEM((32, 128), BF16),
+            pltpu.VMEM((32, 128), BF16),
+            pltpu.VMEM((2, 2, 32), BF16),
+            pltpu.VMEM((2, 2, 32), BF16),
+            pltpu.VMEM((1, 64), F32),
+            pltpu.VMEM((32, 128), BF16),
+            pltpu.VMEM((32, 128), BF16),
+            pltpu.SMEM((2,), F32),
+            pltpu.SMEM((2, 2), F32),
+            pltpu.SMEM((2, 2), F32),
             pltpu.VMEM((4, 256, 256), BF16),
             pltpu.VMEM((4, 256, 256), BF16),
             pltpu.VMEM((2, 32, 640), BF16),
@@ -510,14 +555,10 @@
             pltpu.VMEM((32, 1024), F32),
             pltpu.SemaphoreType.DMA((COPIES,)),
             pltpu.SemaphoreType.DMA((COPIES,)),
-            pltpu.SemaphoreType.DMA((2,)),
+            pltpu.SemaphoreType.DMA((18,)),
         ],
         compiler_params=pltpu.CompilerParams(collective_id=0, has_side_effects=True, vmem_limit_bytes=24 * 2**20),
-    )(
-        tokens, norm_gain.reshape(1, -1), attn_query, attn_key, attn_value, delta_query, delta_key, delta_value,
-        delta_gate, beta_weight.transpose(1, 2, 0), decay_weight.transpose(1, 2, 0), out_gain.reshape(1, -1),
-        attn_out.T, delta_out.T, sink_logit, beta_shift, decay_log,
-    )
+    )(*(pltpu.with_memory_space_constraint(operand, pltpu.HBM) for operand in operands))
     return summed.astype(BF16)
 
 

time: 64.8 us -> 47.8 us (0.74)
  local copies, waits for them, and re-layouts: 9.8 us -> 0 us
  Pallas kernels: 53.6 us -> 47 us
    unnamed x34 -> x0, local copies, waits for them, and re-layouts: 9.8 us -> none
    pallas_call x1, Pallas kernels: 53.6 us -> 47 us  [per_device(): pl.pallas_call(layer_kernel, out_shape=jax.ShapeDtypeStruct((32, 1024), F...]
where the time goes in v3:
time: 47.8 us; the launch traced here: 47.7 us
  Pallas kernels  47 us (98%)
  other arithmetic  0.64 us (1%)
    pallas_call x1, Pallas kernels, per_device(): pl.pallas_call(layer_kernel, out_shape=jax.ShapeDtypeStruct((32, 1024), F...  47 us

profile of v3, /device:TPU:1, one launch (start us, length us, event | category | flops | bytes accessed | tf_op | source)
XLA Modules:
  0.0 47.7 jit_solution(8001491307609154950)
XLA Ops:
  0.0 47.0 %shard_map.163 = f32[32,1024]{1,0:T(8,128)S(1)} custom-call(bf16[128,256]{1,0:T(8,128)(2,1)} %tokens_in.1, f32[1,1024]{1,0:T(1,128)} %bitcast.8, bf16[32,128]{1,0:T(8,128)(2,1)} %aq_in.1, bf16[32,64]{1,0:T(8,128)(2,1)} %ak_in.1, bf16[32,64]{1,0:T(8,128)(2,1)} %av_in.1, bf16[32,128]{1,0:T(8,128)(2,1)} %dq_in.1, bf16[32,128]{1,0:T(8,128)(2,1)} %dk_in.1, ...), custom_call_target="tpu_custom_call" | custom-call | tf_op jit(solution)/shard_map/pallas_call | solution.py:522
  47.1 0.6 %convert_element_type.3 = bf16[32,1024]{1,0:T(8,128)(2,1)} convert(f32[32,1024]{1,0:T(8,128)S(1)} %shard_map.163) | non-fusion elementwise | flops 32768 | bytes 196608 | tf_op jit(solution)/shard_map/convert_element_type | solution.py:562

commit v4 on v3

--- a/solution.py
+++ b/solution.py
@@ -153,64 +153,44 @@
     phase("barrier")
     pl.semaphore_wait(barrier, len(peers))
 
-    class Ring:
+    class Gather:
         def __init__(self, w, s, y_first, source=None):
             self.w, self.s, self.y_first, self.source = w, s, y_first, source
             self.waits = {}
 
-        def slot(self, first, second, half=None):
+        def slot(self, first, second):
             zz, yy = (z + second, y + first) if self.y_first else (z + first, y + second)
-            ref = self.w.at[m4(zz), m4(yy), self.s]
-            return ref if half is None else ref.at[pl.ds(16 * half, 16)]
-
-        def twin(self, _):
-            return self.w.at[z, y, 1 - self.s]
-
-        def dev1(self, d, core=c):
-            return dev_y(d, core) if self.y_first else dev_z(d, core)
-
-        def dev2(self, d, core=c):
-            return dev_z(d, core) if self.y_first else dev_y(d, core)
+            return self.w.at[m4(zz), m4(yy), self.s]
+
+        def own(self, device):
+            if self.source is None:
+                return self.slot(0, 0), self.slot(0, 0), device(c)
+            return self.source, self.w.at[z, y, 1 - self.s], device(o)
+
+        def along(self, axis, d, core):
+            return dev_y(d, core) if axis == self.y_first else dev_z(d, core)
+
+        def begin(self):
+            for d in (1, 3, 2):
+                source, place, device = self.own(lambda core, d=d: self.along(True, d, core))
+                self.waits[d] = send(source, place, device, self.slot(-d, 0))
 
         def across(self, f):
-            for d in (1, -1):
-                if f == 0 and self.source is not None:
-                    self.waits[f, d] = send(self.source, self.twin(0), self.dev2(d, o), self.slot(f, -d))
+            for d in (1, 3, 2):
+                if f == 0:
+                    source, place, device = self.own(lambda core, d=d: self.along(False, d, core))
                 else:
-                    block = self.slot(f, 0)
-                    self.waits[f, d] = send(block, block, self.dev2(d), self.slot(f, -d))
-
-        def relay(self, f):
-            for d, half in ((1, 0), (-1, 1)):
-                self.waits[f, d].wait_recv()
-                block = self.slot(f, -d, half)
-                self.waits[f, 2 * d] = send(block, block, self.dev2(d), self.slot(f, -2 * d, half))
-
-        def begin(self):
-            block = self.slot(0, 0)
-            for d in (1, -1):
-                if self.source is not None:
-                    self.waits[d] = send(self.source, self.twin(0), self.dev1(d, o), self.slot(-d, 0))
-                else:
-                    self.waits[d] = send(block, block, self.dev1(d), self.slot(-d, 0))
-
-        def near(self):
-            for d, half in ((1, 0), (-1, 1)):
-                self.waits[d].wait_recv()
-                block = self.slot(-d, 0, half)
-                self.waits[2 * d] = send(block, block, self.dev1(d), self.slot(-2 * d, 0, half))
-            self.across(-1)
-            self.across(1)
-
-        def far(self):
-            self.waits[2].wait_recv()
-            self.waits[-2].wait_recv()
-            self.across(2)
+                    source, place, device = self.slot(f, 0), self.slot(f, 0), self.along(False, d, c)
+                self.waits[f, d] = send(source, place, device, self.slot(f, -d))
+
+        def forward(self, d):
+            self.waits[d].wait_recv()
+            self.across(-d)
 
         def finish(self):
-            for f in (0, -1, 1, 2):
-                self.waits[f, 2].wait_recv()
-                self.waits[f, -2].wait_recv()
+            for d in (1, 3, 2):
+                for f in (0, -1, -3, -2):
+                    self.waits[f, d].wait_recv()
 
     in_cols = pl.ds(0, 512)
     out_cols = pl.ds(512, 128)
@@ -220,10 +200,10 @@
         return pl.ds(pl.multiple_of(128 * m4(x + d), 128), 128)
 
     phase("start")
-    first = Ring(w1, c, True)
-    second = Ring(w1, o, False, stage.at[o, :, in_cols])
-    out_first = Ring(w2, c, True)
-    out_second = Ring(w2, o, False)
+    first = Gather(w1, c, True)
+    second = Gather(w1, o, False, stage.at[o, :, in_cols])
+    out_first = Gather(w2, c, True)
+    out_second = Gather(w2, o, False)
     first.begin()
     second.begin()
     first.across(0)
@@ -245,19 +225,14 @@
         for d in (1, 3, 2)
     ]
     phase("near")
-    first.near()
-    second.near()
+    for d in (1, 3, 2):
+        first.forward(d)
+        second.forward(d)
     phase("tokens")
     for d, arrived in zip((1, 3, 2), tok_in):
         arrived.wait_recv()
         src = m4(x - d)
         tok_swap.append(send(tok.at[src, half_rows], tok.at[src, half_rows], partner, tok.at[src, other_rows]))
-    phase("relay0")
-    first.relay(0)
-    second.relay(0)
-    phase("far")
-    first.far()
-    second.far()
     phase("tokswap")
     for arrived in tok_swap:
         arrived.wait_recv()
@@ -271,13 +246,7 @@
     for k in range(4):
         normed[k] = (tok[k].astype(F32) * inv * gain[:, 256 * k : 256 * k + 256]).astype(BF16)
 
-    phase("relay1")
-    for f in (-1, 1):
-        first.relay(f)
-        second.relay(f)
-    phase("relay2")
-    first.relay(2)
-    second.relay(2)
+    phase("w2in")
     for arrived in w2_in:
         arrived.wait_recv()
     for ring in (out_first, out_second):
@@ -291,6 +260,11 @@
     proj = mm(normed[0], w1[0].reshape(256, 512))
     for k in range(1, 4):
         proj = proj + mm(normed[k], w1[k].reshape(256, 512))
+    phase("rings")
+    for d in (1, 3, 2):
+        out_first.forward(d)
+        out_second.forward(d)
+    phase("gates0")
     t0, t1, t2 = proj[:, 0:128], proj[:, 128:256], proj[:, 256:384]
     kv[64:320, :] = proj[:, 384:512].astype(BF16)
     halo = [
@@ -339,10 +313,6 @@
     q3 = jnp.concatenate([q_h, q_h, q_l], axis=1)
     key3 = jnp.concatenate([key_h, key_h, key_l], axis=1)
     kt3 = jnp.concatenate([kt_h, kt_l, kt_h], axis=0)
-
-    phase("rings1")
-    out_first.near()
-    out_second.near()
 
     phase("delta1")
     lane2 = lax.broadcasted_iota(jnp.int32, (64, 128), 1)
@@ -399,11 +369,6 @@
     phase("scan1send")
     scan1 = [send(mats.at[y], mats.at[y], dev_y(d), mats.at[m4(y - d)]) for d in (1, 3, 2)]
 
-    phase("rings2")
-    out_first.relay(0)
-    out_second.relay(0)
-    out_first.far()
-    out_second.far()
     phase("reads")
     local, reads = {}, {}
     for way, h in chains:
@@ -452,11 +417,13 @@
             jnp.where(place == 0, eye2, jnp.where(place == 1, m[0], jnp.where(place == 2, two, three)))
         )
     phase("scan2send")
-    scan2 = [send(rowmats.at[z], rowmats.at[z], dev_z(d), rowmats.at[m4(z - d)]) for d in (1, 3, 2)]
-    phase("rings3")
-    for f in (-1, 1, 2):
-        out_first.relay(f)
-        out_second.relay(f)
+    scan2 = []
+    for d in (1, 3, 2):
+        goes = jnp.where(z + d < 4, 0, 1)
+        comes = jnp.where(z - d >= 0, 0, 1)
+        scan2.append(
+            send(rowmats.at[z, goes], rowmats.at[z, goes], dev_z(d), rowmats.at[m4(z - d), comes])
+        )
     phase("scan2wait")
     for arrived in scan2:
         arrived.wait_recv()
@@ -465,11 +432,14 @@
     for way in range(2):
         m = [rowmats[k if way == 0 else 3 - k, way].astype(F32) + eye2 for k in range(3)]
         place = z if way == 0 else 3 - z
-        s1 = m[0][:, 0:64]
-        s2 = dot3_deep(m[1][:, 64:128], s1) + m[1][:, 0:64]
-        s3 = dot3_deep(m[2][:, 64:128], s2) + m[2][:, 0:64]
-        s = jnp.where(place == 0, 0.0, jnp.where(place == 1, s1, jnp.where(place == 2, s2, s3)))
-        states.append(dot3_deep(entry[way][:, 64:128], s) + entry[way][:, 0:64])
+        none = jnp.zeros((64, 64), F32)
+        two = dot3_deep(m[1][:, 64:128], m[0][:, 0:64]) + m[1][:, 0:64]
+        before = jnp.where(place == 3, two, jnp.where(place == 2, m[0][:, 0:64], none))
+        last_map = jnp.where(
+            place == 3, m[2], jnp.where(place == 2, m[1], jnp.where(place == 1, m[0], eye2))
+        )
+        joined = after(entry[way], last_map)
+        states.append(dot3_deep(joined[:, 64:128], before) + joined[:, 0:64])
 
     reads_h, reads_l = split(reads_all)
     states_h, states_l = split(jnp.concatenate(states, axis=0))

time: 47.8 us -> 43.8 us (0.916)
  Pallas kernels: 47 us -> 43 us
    pallas_call x1, Pallas kernels: 47 us -> 43 us  [per_device(): pl.pallas_call(layer_kernel, out_shape=jax.ShapeDtypeStruct((32, 1024), F...]
where the time goes in v4:
time: 43.8 us; the launch traced here: 43.7 us
  Pallas kernels  43 us (98%)
  other arithmetic  0.64 us (1%)
    pallas_call x1, Pallas kernels, per_device(): pl.pallas_call(layer_kernel, out_shape=jax.ShapeDtypeStruct((32, 1024), F...  43 us

profile of v4, /device:TPU:1, one launch (start us, length us, event | category | flops | bytes accessed | tf_op | source)
XLA Modules:
  0.0 43.7 jit_solution(10472073550798118169)
XLA Ops:
  0.0 43.0 %shard_map.163 = f32[32,1024]{1,0:T(8,128)S(1)} custom-call(bf16[128,256]{1,0:T(8,128)(2,1)} %tokens_in.1, f32[1,1024]{1,0:T(1,128)} %bitcast.8, bf16[32,128]{1,0:T(8,128)(2,1)} %aq_in.1, bf16[32,64]{1,0:T(8,128)(2,1)} %ak_in.1, bf16[32,64]{1,0:T(8,128)(2,1)} %av_in.1, bf16[32,128]{1,0:T(8,128)(2,1)} %dq_in.1, bf16[32,128]{1,0:T(8,128)(2,1)} %dk_in.1, ...), custom_call_target="tpu_custom_call" | custom-call | tf_op jit(solution)/shard_map/pallas_call | solution.py:492
  43.0 0.6 %convert_element_type.3 = bf16[32,1024]{1,0:T(8,128)(2,1)} convert(f32[32,1024]{1,0:T(8,128)S(1)} %shard_map.163) | non-fusion elementwise | flops 32768 | bytes 196608 | tf_op jit(solution)/shard_map/convert_element_type | solution.py:532

commit v5 on v4

--- a/solution.py
+++ b/solution.py
@@ -14,7 +14,7 @@
 MESH = pl.DeviceIdType.MESH
 F32 = jnp.float32
 BF16 = jnp.bfloat16
-LINK = F32
+LINK = BF16
 NN = (((1,), (0,)), ((), ()))
 NT = (((1,), (1,)), ((), ()))
 
@@ -60,7 +60,7 @@
     sink_in, shift_in, dlog_in,
     out,
     gain, aq, ak, av, dq, dk, dv, dz, bw, gw, ogain, ao, do, sink, shift, dlog,
-    tok, normed, stage, w1, w2, kv, mats, rowmats, hsend, hall, pbuf, prec, send_sem, recv_sem, own_sem,
+    tok, normed, stage, w1, w2, kv, own_map, maps_in, hsend, hall, pbuf, prec, send_sem, recv_sem, own_sem,
 ):
     sp = lax.axis_index("sp")
     x = lax.axis_index("tp")
@@ -132,7 +132,6 @@
     peers = [partner]
     for d in (1, 2, 3):
         peers += [dev_x(d), dev_y(d), dev_z(d), dev_y(d, o), dev_z(d, o)]
-    peers += [dev_b(1), dev_b(-1)]
     for peer in peers:
         pl.semaphore_signal(barrier, inc=1, device_id=peer, device_id_type=MESH)
     for load in loads[:11]:
@@ -149,6 +148,7 @@
             axis=1,
         )
     w1[z, y, c] = stage[c, :, 0:512]
+    w2[x, z, y, c] = stage[c, :, 512:640]
 
     phase("barrier")
     pl.semaphore_wait(barrier, len(peers))
@@ -194,16 +194,11 @@
 
     in_cols = pl.ds(0, 512)
     out_cols = pl.ds(512, 128)
-    x_cols = pl.ds(pl.multiple_of(128 * x, 128), 128)
-
-    def x_cols_of(d):
-        return pl.ds(pl.multiple_of(128 * m4(x + d), 128), 128)
-
     phase("start")
     first = Gather(w1, c, True)
     second = Gather(w1, o, False, stage.at[o, :, in_cols])
-    out_first = Gather(w2, c, True)
-    out_second = Gather(w2, o, False)
+    out_first = Gather(w2.at[x], c, True)
+    out_second = Gather(w2.at[x], o, False, stage.at[o, :, out_cols])
     first.begin()
     second.begin()
     first.across(0)
@@ -213,21 +208,14 @@
     tok_in = [send(tokens, tokens, dev_x(d), tok.at[m4(x - d), half_rows]) for d in (1, 3, 2)]
     w_swap = send(stage.at[o, :, in_cols], w1.at[z, y, c], partner, w1.at[z, y, o])
     tok_swap = [send(tokens, tokens, partner, tok.at[x, other_rows])]
-    w2_swap = send(stage.at[o, :, out_cols], w2.at[z, y, c, :, x_cols], partner, w2.at[z, y, o, :, x_cols])
-    own_w2 = pltpu.make_async_copy(stage.at[c, :, out_cols], w2.at[z, y, c, :, x_cols], own_sem.at[17])
-    own_w2.start()
-    phase("swap")
-    w_swap.wait_recv()
-    own_w2.wait()
-    w2_swap.wait_recv()
-    w2_in = [
-        send(w2.at[z, y, :, :, x_cols], w2.at[z, y, :, :, x_cols], dev_x(d), w2.at[z, y, :, :, x_cols_of(-d)])
-        for d in (1, 3, 2)
-    ]
+    w2_swap = send(stage.at[o, :, out_cols], w2.at[x, z, y, c], partner, w2.at[x, z, y, o])
     phase("near")
     for d in (1, 3, 2):
         first.forward(d)
         second.forward(d)
+    for ring in (out_first, out_second):
+        ring.begin()
+        ring.across(0)
     phase("tokens")
     for d, arrived in zip((1, 3, 2), tok_in):
         arrived.wait_recv()
@@ -246,13 +234,12 @@
     for k in range(4):
         normed[k] = (tok[k].astype(F32) * inv * gain[:, 256 * k : 256 * k + 256]).astype(BF16)
 
-    phase("w2in")
-    for arrived in w2_in:
-        arrived.wait_recv()
-    for ring in (out_first, out_second):
-        ring.begin()
-        ring.across(0)
+    phase("w2near")
+    for d in (1, 3, 2):
+        out_first.forward(d)
+        out_second.forward(d)
     phase("wfinish")
+    w_swap.wait_recv()
     first.finish()
     second.finish()
 
@@ -260,10 +247,6 @@
     proj = mm(normed[0], w1[0].reshape(256, 512))
     for k in range(1, 4):
         proj = proj + mm(normed[k], w1[k].reshape(256, 512))
-    phase("rings")
-    for d in (1, 3, 2):
-        out_first.forward(d)
-        out_second.forward(d)
     phase("gates0")
     t0, t1, t2 = proj[:, 0:128], proj[:, 128:256], proj[:, 256:384]
     kv[64:320, :] = proj[:, 384:512].astype(BF16)
@@ -314,6 +297,11 @@
     key3 = jnp.concatenate([key_h, key_h, key_l], axis=1)
     kt3 = jnp.concatenate([kt_h, kt_l, kt_h], axis=0)
 
+    phase("rings")
+    w2_swap.wait_recv()
+    out_first.finish()
+    out_second.finish()
+    w2_in = [send(w2.at[x], w2.at[x], dev_x(d), w2.at[m4(x - d)]) for d in (1, 3, 2)]
     phase("delta1")
     lane2 = lax.broadcasted_iota(jnp.int32, (64, 128), 1)
     row2 = lax.broadcasted_iota(jnp.int32, (64, 128), 0)
@@ -357,18 +345,23 @@
     phase("final")
 
     def after(later, earlier):
-        return dot3_deep(later[:, 64:128], earlier) + jnp.where(lane2 < 64, later, 0.0)
+        return dot3_deep(later[:, 64:128], earlier) + later + earlier
 
     maps = {}
     for at in chains:
         final = dot3(key_end[at], uw[at])
-        maps[at] = jnp.where(lane2 < 64, final, end[at] * eye2 - final)
+        maps[at] = jnp.where(lane2 < 64, final, (end[at] - 1.0) * eye2 - final)
     for way in range(2):
-        block_map = after(maps[way, 1 - way], maps[way, way])
-        mats[y, way] = (block_map - eye2).astype(LINK)
+        own_map[way] = after(maps[way, 1 - way], maps[way, way]).astype(LINK)
     phase("scan1send")
-    scan1 = [send(mats.at[y], mats.at[y], dev_y(d), mats.at[m4(y - d)]) for d in (1, 3, 2)]
-
+    scan = []
+    steps = [(dz, dy) for dz in range(4) for dy in range(4) if (dz, dy) != (0, 0)]
+    for dz, dy in sorted(steps, key=lambda step: -(min(step[0], 4 - step[0]) + min(step[1], 4 - step[1]))):
+        zz, yy = m4(z + dz), m4(y + dy)
+        goes = jnp.where(zz * 4 + yy > b, 0, 1)
+        scan.append(
+            send(own_map.at[goes], maps_in.at[z, y], dev(zz, yy, c, x), maps_in.at[m4(z - dz), m4(y - dy)])
+        )
     phase("reads")
     local, reads = {}, {}
     for way, h in chains:
@@ -379,7 +372,7 @@
         if h != way:
             passed = dot3_deep(reads[at], maps[way, way])
             local[at] = local[at] + passed[:, 0:64]
-            reads[at] = passed[:, 64:128]
+            reads[at] = reads[at] + passed[:, 64:128]
     local_sum = jnp.concatenate([local[0, h] + local[1, h] for h in range(2)], axis=0)
     reads_all = jnp.concatenate(
         [jnp.concatenate([reads[0, h], reads[1, h]], axis=1) for h in range(2)], axis=0
@@ -401,45 +394,26 @@
     weights = (weights / total).astype(BF16)
     attn_heads = mm(weights, kv[:, 64:128])
 
-    phase("scan1wait")
-    for arrived in scan1:
-        arrived.wait_recv()
-
-    phase("compose")
-    entry = []
-    for way in range(2):
-        m = [mats[k if way == 0 else 3 - k, way].astype(F32) + eye2 for k in range(4)]
-        place = y if way == 0 else 3 - y
-        two = after(m[1], m[0])
-        three = after(m[2], two)
-        rowmats[z, way] = (after(after(m[3], m[2]), two) - eye2).astype(LINK)
-        entry.append(
-            jnp.where(place == 0, eye2, jnp.where(place == 1, m[0], jnp.where(place == 2, two, three)))
-        )
-    phase("scan2send")
-    scan2 = []
-    for d in (1, 3, 2):
-        goes = jnp.where(z + d < 4, 0, 1)
-        comes = jnp.where(z - d >= 0, 0, 1)
-        scan2.append(
-            send(rowmats.at[z, goes], rowmats.at[z, goes], dev_z(d), rowmats.at[m4(z - d), comes])
-        )
-    phase("scan2wait")
-    for arrived in scan2:
+    phase("scanwait")
+    for arrived in scan:
         arrived.wait_recv()
     phase("states")
     states = []
     for way in range(2):
-        m = [rowmats[k if way == 0 else 3 - k, way].astype(F32) + eye2 for k in range(3)]
-        place = z if way == 0 else 3 - z
-        none = jnp.zeros((64, 64), F32)
-        two = dot3_deep(m[1][:, 64:128], m[0][:, 0:64]) + m[1][:, 0:64]
-        before = jnp.where(place == 3, two, jnp.where(place == 2, m[0][:, 0:64], none))
-        last_map = jnp.where(
-            place == 3, m[2], jnp.where(place == 2, m[1], jnp.where(place == 1, m[0], eye2))
-        )
-        joined = after(entry[way], last_map)
-        states.append(dot3_deep(joined[:, 64:128], before) + joined[:, 0:64])
+        order = range(16) if way == 0 else range(15, -1, -1)
+        chain = []
+        for k in order:
+            inside = (b > k) if way == 0 else (b < k)
+            chain.append(jnp.where(inside, maps_in[k // 4, k % 4], jnp.zeros((64, 128), LINK)))
+        level = []
+        for k in range(0, 14, 2):
+            earlier, later = chain[k], chain[k + 1]
+            level.append(mm(later[:, 64:128], earlier) + later.astype(F32) + earlier.astype(F32))
+        level.append(chain[14].astype(F32))
+        while len(level) > 2:
+            level = [after(level[k + 1], level[k]) for k in range(0, len(level), 2)]
+        start = level[0][:, 0:64]
+        states.append(dot3_deep(level[1][:, 64:128], start) + start + level[1][:, 0:64])
 
     reads_h, reads_l = split(reads_all)
     states_h, states_l = split(jnp.concatenate(states, axis=0))
@@ -450,6 +424,7 @@
     whole = local_sum + whole + mm(reads_h, states_l)
     scaled = whole * lax.rsqrt(jnp.mean(whole * whole, axis=-1, keepdims=True) + EPS) * ogain[...]
     heads = jnp.concatenate([attn_heads, scaled * gate], axis=1).astype(BF16)
+    phase("headsend0")
     for k in range(4):
         hsend[k, 0:32] = heads[32 * k : 32 * k + 32]
         hsend[k, 32:64] = heads[128 + 32 * k : 160 + 32 * k]
@@ -457,15 +432,16 @@
     head_in = [send(hsend.at[m4(x + d)], hall.at[x], dev_x(d), hall.at[m4(x - d)]) for d in (1, 3, 2)]
     hall[x] = hsend[x]
     phase("w2finish")
-    out_first.finish()
-    out_second.finish()
+    for arrived in w2_in:
+        arrived.wait_recv()
     phase("headwait")
     for arrived in head_in:
         arrived.wait_recv()
     phase("outmm")
     gathered = jnp.concatenate([hall[k] for k in range(4)], axis=1)
     for k in range(4):
-        part = mm(gathered, w2[k].reshape(256, 512), NT)
+        rows = jnp.concatenate([w2[kx, k].reshape(256, 128) for kx in range(4)], axis=1)
+        part = mm(gathered, rows, NT)
         pbuf[0, :, 256 * k : 256 * k + 256] = part[0:32]
         pbuf[1, :, 256 * k : 256 * k + 256] = part[32:64]
     phase("last")
@@ -515,10 +491,10 @@
             pltpu.VMEM((4, 256, 256), BF16),
             pltpu.VMEM((2, 32, 640), BF16),
             pltpu.VMEM((4, 4, 2, 32, 512), BF16),
-            pltpu.VMEM((4, 4, 2, 32, 512), BF16),
+            pltpu.VMEM((4, 4, 4, 2, 32, 128), BF16),
             pltpu.VMEM((384, 128), BF16),
-            pltpu.VMEM((4, 2, 64, 128), LINK),
-            pltpu.VMEM((4, 2, 64, 128), LINK),
+            pltpu.VMEM((2, 64, 128), LINK),
+            pltpu.VMEM((4, 4, 64, 128), LINK),
             pltpu.VMEM((4, 64, 128), BF16),
             pltpu.VMEM((4, 64, 128), BF16),
             pltpu.VMEM((2, 32, 1024), F32),

time: 43.8 us -> 44.4 us (1.014)
  Pallas kernels: 43 us -> 43.6 us
    pallas_call x1, Pallas kernels: 43 us -> 43.6 us  [per_device(): pl.pallas_call(layer_kernel, out_shape=jax.ShapeDtypeStruct((32, 1024), F...]
where the time goes in v5:
time: 44.4 us; the launch traced here: 44.2 us
  Pallas kernels  43.6 us (98%)
  other arithmetic  0.64 us (1%)
    pallas_call x1, Pallas kernels, per_device(): pl.pallas_call(layer_kernel, out_shape=jax.ShapeDtypeStruct((32, 1024), F...  43.6 us

profile of v5, /device:TPU:1, one launch (start us, length us, event | category | flops | bytes accessed | tf_op | source)
XLA Modules:
  0.0 44.2 jit_solution(14564345894349576866)
XLA Ops:
  0.0 43.6 %shard_map.163 = f32[32,1024]{1,0:T(8,128)S(1)} custom-call(bf16[128,256]{1,0:T(8,128)(2,1)} %tokens_in.1, f32[1,1024]{1,0:T(1,128)} %bitcast.8, bf16[32,128]{1,0:T(8,128)(2,1)} %aq_in.1, bf16[32,64]{1,0:T(8,128)(2,1)} %ak_in.1, bf16[32,64]{1,0:T(8,128)(2,1)} %av_in.1, bf16[32,128]{1,0:T(8,128)(2,1)} %dq_in.1, bf16[32,128]{1,0:T(8,128)(2,1)} %dk_in.1, ...), custom_call_target="tpu_custom_call" | custom-call | tf_op jit(solution)/shard_map/pallas_call | solution.py:468
  43.6 0.6 %convert_element_type.3 = bf16[32,1024]{1,0:T(8,128)(2,1)} convert(f32[32,1024]{1,0:T(8,128)S(1)} %shard_map.163) | non-fusion elementwise | flops 32768 | bytes 196608 | tf_op jit(solution)/shard_map/convert_element_type | solution.py:508

commit v6 on v5

--- a/solution.py
+++ b/solution.py
@@ -45,10 +45,18 @@
     return both[:, 0:128] + both[:, 128:256]
 
 
-def dot3_deep(a, b):
-    ah, al = split(a)
-    bh, bl = split(b)
-    return mm(jnp.concatenate([ah, ah, al], axis=1), jnp.concatenate([bh, bl, bh], axis=0))
+def right64(b):
+    hi, lo = split(b)
+    none = jnp.zeros_like(lo)
+    blank = jnp.concatenate([none, none], axis=1)
+    return jnp.concatenate(
+        [jnp.concatenate([hi, lo], axis=1), blank, jnp.concatenate([hi, none], axis=1), blank], axis=0
+    )
+
+
+def dot64(a, b):
+    both = mm(left(a), right64(b))
+    return both[:, 0:128] + both[:, 128:256]
 
 
 def silu(v):
@@ -143,7 +151,7 @@
         cols = slice(64 * cc, 64 * cc + 64)
         small = jnp.concatenate([bw[cc].astype(F32), gw[cc].astype(F32), blank], axis=0).T.astype(BF16)
         stage[cc] = jnp.concatenate(
-            [aq[:, cols], dq[:, cols], dk[:, cols], dv[:, cols], dz[:, cols], small, ak[...], av[...],
+            [dq[:, cols], aq[:, cols], dk[:, cols], dv[:, cols], dz[:, cols], small, av[...], ak[...],
              attn_t[:, cols], delta_t[:, cols]],
             axis=1,
         )
@@ -154,58 +162,57 @@
     pl.semaphore_wait(barrier, len(peers))
 
     class Gather:
-        def __init__(self, w, s, y_first, source=None):
-            self.w, self.s, self.y_first, self.source = w, s, y_first, source
+        def __init__(self, place, y_first, source=None, twin=None):
+            self.place, self.y_first, self.source, self.twin = place, y_first, source, twin
             self.waits = {}
 
         def slot(self, first, second):
             zz, yy = (z + second, y + first) if self.y_first else (z + first, y + second)
-            return self.w.at[m4(zz), m4(yy), self.s]
-
-        def own(self, device):
+            return self.place(m4(zz), m4(yy))
+
+        def own(self, axis, d):
+            device = dev_y if axis == self.y_first else dev_z
             if self.source is None:
-                return self.slot(0, 0), self.slot(0, 0), device(c)
-            return self.source, self.w.at[z, y, 1 - self.s], device(o)
-
-        def along(self, axis, d, core):
-            return dev_y(d, core) if axis == self.y_first else dev_z(d, core)
+                return self.slot(0, 0), self.slot(0, 0), device(d)
+            return self.source, self.twin, device(d, o)
 
         def begin(self):
             for d in (1, 3, 2):
-                source, place, device = self.own(lambda core, d=d: self.along(True, d, core))
-                self.waits[d] = send(source, place, device, self.slot(-d, 0))
-
-        def across(self, f):
+                self.waits[d] = send(*self.own(True, d), self.slot(-d, 0))
             for d in (1, 3, 2):
-                if f == 0:
-                    source, place, device = self.own(lambda core, d=d: self.along(False, d, core))
-                else:
-                    source, place, device = self.slot(f, 0), self.slot(f, 0), self.along(False, d, c)
-                self.waits[f, d] = send(source, place, device, self.slot(f, -d))
+                self.waits[0, d] = send(*self.own(False, d), self.slot(0, -d))
 
         def forward(self, d):
             self.waits[d].wait_recv()
-            self.across(-d)
+            block = self.slot(-d, 0)
+            for e in (1, 3, 2):
+                device = dev_z(e) if self.y_first else dev_y(e)
+                self.waits[-d, e] = send(block, block, device, self.slot(-d, -e))
 
         def finish(self):
-            for d in (1, 3, 2):
+            for e in (1, 3, 2):
                 for f in (0, -1, -3, -2):
-                    self.waits[f, d].wait_recv()
+                    self.waits[f, e].wait_recv()
 
     in_cols = pl.ds(0, 512)
     out_cols = pl.ds(512, 128)
     phase("start")
-    first = Gather(w1, c, True)
-    second = Gather(w1, o, False, stage.at[o, :, in_cols])
-    out_first = Gather(w2.at[x], c, True)
-    out_second = Gather(w2.at[x], o, False, stage.at[o, :, out_cols])
+    first = Gather(lambda zz, yy: w1.at[zz, yy, c], True)
+    second = Gather(lambda zz, yy: w1.at[zz, yy, o], False, stage.at[o, :, in_cols], w1.at[z, y, c])
+    out_low = Gather(lambda zz, yy: w2.at[:, zz, yy, c, pl.ds(0, 16)], True)
+    out_high = Gather(lambda zz, yy: w2.at[:, zz, yy, c, pl.ds(16, 16)], False)
+    out_twin = Gather(
+        lambda zz, yy: w2.at[x, zz, yy, o], False, stage.at[o, :, out_cols], w2.at[x, z, y, c]
+    )
     first.begin()
     second.begin()
-    first.across(0)
-    second.across(0)
+    out_twin.begin()
     for load in loads[11:]:
         load.wait()
     tok_in = [send(tokens, tokens, dev_x(d), tok.at[m4(x - d), half_rows]) for d in (1, 3, 2)]
+    w2_own = [
+        send(stage.at[c, :, out_cols], w2.at[x, z, y, c], dev_x(d), w2.at[m4(x - d), z, y, c]) for d in (1, 3, 2)
+    ]
     w_swap = send(stage.at[o, :, in_cols], w1.at[z, y, c], partner, w1.at[z, y, o])
     tok_swap = [send(tokens, tokens, partner, tok.at[x, other_rows])]
     w2_swap = send(stage.at[o, :, out_cols], w2.at[x, z, y, c], partner, w2.at[x, z, y, o])
@@ -213,9 +220,12 @@
     for d in (1, 3, 2):
         first.forward(d)
         second.forward(d)
-    for ring in (out_first, out_second):
-        ring.begin()
-        ring.across(0)
+    for d in (1, 3, 2):
+        out_twin.forward(d)
+    for arrived in w2_own:
+        arrived.wait_recv()
+    out_low.begin()
+    out_high.begin()
     phase("tokens")
     for d, arrived in zip((1, 3, 2), tok_in):
         arrived.wait_recv()
@@ -234,10 +244,6 @@
     for k in range(4):
         normed[k] = (tok[k].astype(F32) * inv * gain[:, 256 * k : 256 * k + 256]).astype(BF16)
 
-    phase("w2near")
-    for d in (1, 3, 2):
-        out_first.forward(d)
-        out_second.forward(d)
     phase("wfinish")
     w_swap.wait_recv()
     first.finish()
@@ -254,16 +260,16 @@
         send(kv.at[pl.ds(256, 64)], kv.at[pl.ds(0, 64)], dev_b(1), kv.at[pl.ds(0, 64)]),
         send(kv.at[pl.ds(64, 64)], kv.at[pl.ds(320, 64)], dev_b(-1), kv.at[pl.ds(320, 64)]),
     ]
-    att_q = t0[:, 0:64].astype(BF16)
-    act_q = silu(t0[:, 64:128].astype(BF16).astype(F32))
-    act_kv = silu(t1.astype(BF16).astype(F32))
-    act_k, val = act_kv[:, 0:64], act_kv[:, 64:128]
-    q = act_q * lax.rsqrt(jnp.sum(act_q * act_q, axis=-1, keepdims=True) + EPS) * HEAD_DIM**-0.5
-    key = act_k * lax.rsqrt(jnp.sum(act_k * act_k, axis=-1, keepdims=True) + EPS)
-    gate = silu(t2[:, 0:64].astype(BF16).astype(F32))
+    lane = lax.broadcasted_iota(jnp.int32, (1, 128), 1)
+    head = lane < 64
+    act = silu(t0.astype(BF16).astype(F32))
+    act = jnp.where(head, act, 0.0)
+    q = act * (lax.rsqrt(jnp.sum(act * act, axis=-1, keepdims=True) + EPS) * HEAD_DIM**-0.5)
+    act = silu(t1.astype(BF16).astype(F32))
+    act_k = jnp.where(head, act, 0.0)
+    key_val = jnp.where(head, act * lax.rsqrt(jnp.sum(act_k * act_k, axis=-1, keepdims=True) + EPS), act)
 
     phase("gates")
-    lane = lax.broadcasted_iota(jnp.int32, (1, 128), 1)
     bias = jnp.where(lane == 64, shift[0, c], jnp.where(lane == 65, shift[1, c], 0.0))
     rate = jnp.exp(jnp.where(lane == 66, dlog[0, c], jnp.where(lane == 67, dlog[1, c], 0.0)))
     strength = jax.nn.sigmoid(t2 + bias)
@@ -281,40 +287,41 @@
     g_mid = rest.astype(BF16)
     g_lo = (rest - g_mid.astype(F32)).astype(BF16)
     g_parts = jnp.concatenate(
-        [part[128 * h : 128 * h + 128, 64:128] for h in range(2) for part in (g_hi, g_mid, g_lo)], axis=1
-    )
-    sums = [mm(jnp.where(mask, 1.0, 0.0).astype(BF16), g_parts) for mask in masks]
-    sub = lax.broadcasted_iota(jnp.int32, (1, 192), 1)
-    picked = jnp.where((sub & 63) == 2, sums[0][:, 0:192], sums[1][:, 0:192])
-    picked2 = jnp.where((sub & 63) == 2, sums[0][:, 192:384], sums[1][:, 192:384])
-    g_all = jnp.concatenate([p[:, 0:64] + p[:, 64:128] + p[:, 128:192] for p in (picked, picked2)], axis=0)
-    turned = jnp.concatenate([key, g_all], axis=1).T
+        [jnp.concatenate([part[0:128], part[128:256]], axis=1) for part in (g_hi, g_mid, g_lo)], axis=0
+    )
+    ones = jnp.concatenate([jnp.where(mask, 1.0, 0.0).astype(BF16) for mask in masks], axis=0)
+    sums = mm(jnp.concatenate([ones, ones, ones], axis=1), g_parts)
+    g_all = jnp.where(
+        lane == 66,
+        jnp.concatenate([sums[0:128, 0:128], sums[0:128, 128:256]], axis=0),
+        jnp.concatenate([sums[128:256, 0:128], sums[128:256, 128:256]], axis=0),
+    )
+    turned = jnp.where(head, key_val, g_all).T
     key_t = turned[0:64]
-    key_h, key_l = split(key)
-    q_h, q_l = split(q)
-    kt_h, kt_l = split(key_t)
-    q3 = jnp.concatenate([q_h, q_h, q_l], axis=1)
-    key3 = jnp.concatenate([key_h, key_h, key_l], axis=1)
-    kt3 = jnp.concatenate([kt_h, kt_l, kt_h], axis=0)
+    q_left, key_left = left(q), left(key_val)
 
     phase("rings")
     w2_swap.wait_recv()
-    out_first.finish()
-    out_second.finish()
-    w2_in = [send(w2.at[x], w2.at[x], dev_x(d), w2.at[m4(x - d)]) for d in (1, 3, 2)]
+    for d in (1, 3, 2):
+        out_low.forward(d)
+        out_high.forward(d)
+    out_twin.finish()
+    w2_in = [send(w2.at[x, :, :, o], w2.at[x, :, :, o], dev_x(d), w2.at[m4(x - d), :, :, o]) for d in (1, 3, 2)]
+
     phase("delta1")
     lane2 = lax.broadcasted_iota(jnp.int32, (64, 128), 1)
     row2 = lax.broadcasted_iota(jnp.int32, (64, 128), 0)
-    eye2 = jnp.where(lane2 == row2 + 64, 1.0, 0.0)
+    eye2 = jnp.where(lane2 == row2, 1.0, 0.0)
     chains = [(way, h) for way in range(2) for h in range(2)]
-    low, scores_d, sides, grown, key_end, end, d = {}, {}, {}, {}, {}, {}, {}
+    low, scores_d, sides, grown, key_end, end = {}, {}, {}, {}, {}, {}
     for h in range(2):
         hs = slice(128 * h, 128 * h + 128)
-        pairs = mm(jnp.concatenate([q3[hs], key3[hs]], axis=0), kt3[:, hs])
+        pairs = mm(jnp.concatenate([q_left[hs], key_left[hs]], axis=0), right64(key_t[:, hs]))
+        pairs = pairs[:, 0:128] + pairs[:, 128:256]
         for way in range(2):
             at = way, h
             beta = strength[hs, 64 + way : 65 + way]
-            g_col = g_all[hs, 2 + way : 3 + way]
+            g_col = g_all[hs, 66 + way : 67 + way]
             g_row = turned[66 + way : 67 + way, hs]
             g_end = g_col[127:128] if way == 0 else g_col[0:1]
             decays = jnp.exp(jnp.where(masks[way], g_col - g_row, -jnp.inf))
@@ -322,7 +329,7 @@
             scores_d[at] = pairs[0:128] * decays
             up = jnp.exp(g_col)
             grown[at] = up * q[hs]
-            sides[at] = jnp.concatenate([beta * val[hs], (beta * up) * key[hs]], axis=1)
+            sides[at] = key_val[hs] * jnp.where(head, beta * up, beta)
             key_end[at] = key_t[:, hs] * jnp.exp(g_end - g_row)
             end[at] = jnp.exp(g_end)
     d1 = {at: jnp.where(near16, low[at], 0.0) for at in chains}
@@ -336,21 +343,21 @@
     inner = {at: inner[at] + dot3(inner[at], d8[at]) for at in chains}
     phase("delta2")
     m1 = {at: dot3(inner[at], off[at]) for at in chains}
-    uw = {at: dot3(inner[at], sides[at]) for at in chains}
+    wu = {at: dot3(inner[at], sides[at]) for at in chains}
     m2 = {at: dot3(m1[at], m1[at]) for at in chains}
-    uw = {at: uw[at] - dot3(m1[at], uw[at]) for at in chains}
+    wu = {at: wu[at] - dot3(m1[at], wu[at]) for at in chains}
     m4_ = {at: dot3(m2[at], m2[at]) for at in chains}
-    uw = {at: uw[at] + dot3(m2[at], uw[at]) for at in chains}
-    uw = {at: uw[at] + dot3(m4_[at], uw[at]) for at in chains}
+    wu = {at: wu[at] + dot3(m2[at], wu[at]) for at in chains}
+    wu = {at: wu[at] + dot3(m4_[at], wu[at]) for at in chains}
     phase("final")
 
     def after(later, earlier):
-        return dot3_deep(later[:, 64:128], earlier) + later + earlier
+        return dot64(later, earlier) + later + earlier
 
     maps = {}
     for at in chains:
-        final = dot3(key_end[at], uw[at])
-        maps[at] = jnp.where(lane2 < 64, final, (end[at] - 1.0) * eye2 - final)
+        final = dot3(key_end[at], wu[at])
+        maps[at] = jnp.where(lane2 < 64, (end[at] - 1.0) * eye2 - final, final)
     for way in range(2):
         own_map[way] = after(maps[way, 1 - way], maps[way, way]).astype(LINK)
     phase("scan1send")
@@ -363,26 +370,26 @@
             send(own_map.at[goes], maps_in.at[z, y], dev(zz, yy, c, x), maps_in.at[m4(z - dz), m4(y - dy)])
         )
     phase("reads")
-    local, reads = {}, {}
+    reads = {}
     for way, h in chains:
         at = way, h
-        read = dot3(scores_d[at], uw[at])
-        local[at] = read[:, 0:64]
-        reads[at] = grown[at] - read[:, 64:128]
+        read = dot3(scores_d[at], wu[at])
+        reads[at] = jnp.where(head, grown[at] - read, read)
         if h != way:
-            passed = dot3_deep(reads[at], maps[way, way])
-            local[at] = local[at] + passed[:, 0:64]
-            reads[at] = reads[at] + passed[:, 64:128]
-    local_sum = jnp.concatenate([local[0, h] + local[1, h] for h in range(2)], axis=0)
-    reads_all = jnp.concatenate(
-        [jnp.concatenate([reads[0, h], reads[1, h]], axis=1) for h in range(2)], axis=0
-    )
+            reads[at] = reads[at] + dot64(reads[at], maps[way, way])
+    reads = [jnp.concatenate([reads[way, 0], reads[way, 1]], axis=0) for way in range(2)]
+    reads_left = [left(r) for r in reads]
+    local = reads[0] + reads[1]
+    gate = silu(t2.astype(BF16).astype(F32))
+    gate = jnp.concatenate([gate[:, 64:128], gate[:, 0:64]], axis=1)
+    gain_row = jnp.concatenate([ogain[...], ogain[...]], axis=1)
 
     phase("halo")
     for arrived in halo:
         arrived.wait_recv()
     phase("attn")
-    scores = mm(att_q, kv[:, 0:64], NT) * HEAD_DIM**-0.5
+    att_q = jnp.where(head, 0.0, t0).astype(BF16)
+    scores = mm(att_q, kv[...], NT) * HEAD_DIM**-0.5
     q_pos = lax.broadcasted_iota(jnp.int32, (ROWS, ROWS + 2 * WINDOW), 0)
     k_pos = lax.broadcasted_iota(jnp.int32, (ROWS, ROWS + 2 * WINDOW), 1) - WINDOW
     seen = k_pos + b * ROWS
@@ -392,7 +399,7 @@
     weights = jnp.exp(scores - top)
     total = jnp.sum(weights, axis=-1, keepdims=True) + jnp.exp(sink[c] - top)
     weights = (weights / total).astype(BF16)
-    attn_heads = mm(weights, kv[:, 64:128])
+    attn_heads = mm(weights, kv[...])
 
     phase("scanwait")
     for arrived in scan:
@@ -408,22 +415,21 @@
         level = []
         for k in range(0, 14, 2):
             earlier, later = chain[k], chain[k + 1]
-            level.append(mm(later[:, 64:128], earlier) + later.astype(F32) + earlier.astype(F32))
+            level.append(
+                mm(later, jnp.concatenate([earlier, jnp.zeros_like(earlier)], axis=0))
+                + later.astype(F32)
+                + earlier.astype(F32)
+            )
         level.append(chain[14].astype(F32))
-        while len(level) > 2:
+        while len(level) > 1:
             level = [after(level[k + 1], level[k]) for k in range(0, len(level), 2)]
-        start = level[0][:, 0:64]
-        states.append(dot3_deep(level[1][:, 64:128], start) + start + level[1][:, 0:64])
-
-    reads_h, reads_l = split(reads_all)
-    states_h, states_l = split(jnp.concatenate(states, axis=0))
-    whole = mm(
-        jnp.concatenate([reads_h, reads_l], axis=1),
-        jnp.concatenate([states_h, states_h], axis=0),
-    )
-    whole = local_sum + whole + mm(reads_h, states_l)
-    scaled = whole * lax.rsqrt(jnp.mean(whole * whole, axis=-1, keepdims=True) + EPS) * ogain[...]
-    heads = jnp.concatenate([attn_heads, scaled * gate], axis=1).astype(BF16)
+        states.append(jnp.where(lane2 < 64, 0.0, level[0]))
+
+    phase("whole")
+    both = mm(reads_left[0], right64(states[0])) + mm(reads_left[1], right64(states[1]))
+    whole = jnp.where(head, 0.0, local + both[:, 0:128] + both[:, 128:256])
+    scaled = whole * lax.rsqrt(jnp.sum(whole * whole, axis=-1, keepdims=True) * (1.0 / HEAD_DIM) + EPS) * gain_row
+    heads = jnp.where(head, attn_heads, scaled * gate).astype(BF16)
     phase("headsend0")
     for k in range(4):
         hsend[k, 0:32] = heads[32 * k : 32 * k + 32]
@@ -432,6 +438,8 @@
     head_in = [send(hsend.at[m4(x + d)], hall.at[x], dev_x(d), hall.at[m4(x - d)]) for d in (1, 3, 2)]
     hall[x] = hsend[x]
     phase("w2finish")
+    out_low.finish()
+    out_high.finish()
     for arrived in w2_in:
         arrived.wait_recv()
     phase("headwait")

time: 44.4 us -> 39.7 us (0.89)
  Pallas kernels: 43.6 us -> 38.9 us
    pallas_call x1, Pallas kernels: 43.6 us -> 38.9 us  [per_device(): pl.pallas_call(layer_kernel, out_shape=jax.ShapeDtypeStruct((32, 1024), F...]
where the time goes in v6:
time: 39.7 us; the launch traced here: 39.6 us
  Pallas kernels  38.9 us (98%)
  other arithmetic  0.64 us (2%)
    pallas_call x1, Pallas kernels, per_device(): pl.pallas_call(layer_kernel, out_shape=jax.ShapeDtypeStruct((32, 1024), F...  38.9 us

profile of v6, /device:TPU:1, one launch (start us, length us, event | category | flops | bytes accessed | tf_op | source)
XLA Modules:
  0.0 39.6 jit_solution(4609852089928735032)
XLA Ops:
  0.0 38.9 %shard_map.163 = f32[32,1024]{1,0:T(8,128)S(1)} custom-call(bf16[128,256]{1,0:T(8,128)(2,1)} %tokens_in.1, f32[1,1024]{1,0:T(1,128)} %bitcast.8, bf16[32,128]{1,0:T(8,128)(2,1)} %aq_in.1, bf16[32,64]{1,0:T(8,128)(2,1)} %ak_in.1, bf16[32,64]{1,0:T(8,128)(2,1)} %av_in.1, bf16[32,128]{1,0:T(8,128)(2,1)} %dq_in.1, bf16[32,128]{1,0:T(8,128)(2,1)} %dk_in.1, ...), custom_call_target="tpu_custom_call" | custom-call | tf_op jit(solution)/shard_map/pallas_call | solution.py:476
  38.9 0.6 %convert_element_type.3 = bf16[32,1024]{1,0:T(8,128)(2,1)} convert(f32[32,1024]{1,0:T(8,128)S(1)} %shard_map.163) | non-fusion elementwise | flops 32768 | bytes 196608 | tf_op jit(solution)/shard_map/convert_element_type | solution.py:516

commit v7 on v6

--- a/solution.py
+++ b/solution.py
@@ -10,7 +10,7 @@
 ROWS = 256
 TOKENS = 4096
 EPS = 1e-6
-COPIES = 120
+COPIES = 168
 MESH = pl.DeviceIdType.MESH
 F32 = jnp.float32
 BF16 = jnp.bfloat16
@@ -68,7 +68,7 @@
     sink_in, shift_in, dlog_in,
     out,
     gain, aq, ak, av, dq, dk, dv, dz, bw, gw, ogain, ao, do, sink, shift, dlog,
-    tok, normed, stage, w1, w2, kv, own_map, maps_in, hsend, hall, pbuf, prec, send_sem, recv_sem, own_sem,
+    tok, normed, stage, w1, wq, wkv, w2, kv, own_map, maps_in, hsend, hall, pbuf, prec, send_sem, recv_sem, own_sem,
 ):
     sp = lax.axis_index("sp")
     x = lax.axis_index("tp")
@@ -151,11 +151,13 @@
         cols = slice(64 * cc, 64 * cc + 64)
         small = jnp.concatenate([bw[cc].astype(F32), gw[cc].astype(F32), blank], axis=0).T.astype(BF16)
         stage[cc] = jnp.concatenate(
-            [dq[:, cols], aq[:, cols], dk[:, cols], dv[:, cols], dz[:, cols], small, av[...], ak[...],
+            [dk[:, cols], dv[:, cols], dz[:, cols], small, dq[:, cols], aq[:, cols], av[...], ak[...],
              attn_t[:, cols], delta_t[:, cols]],
             axis=1,
         )
-    w1[z, y, c] = stage[c, :, 0:512]
+    w1[z, y, c] = stage[c, :, 0:256]
+    wq[z, y, c] = stage[c, :, 256:384]
+    wkv[z, y, c] = stage[c, :, 384:512]
     w2[x, z, y, c] = stage[c, :, 512:640]
 
     phase("barrier")
@@ -179,6 +181,8 @@
         def begin(self):
             for d in (1, 3, 2):
                 self.waits[d] = send(*self.own(True, d), self.slot(-d, 0))
+
+        def across(self):
             for d in (1, 3, 2):
                 self.waits[0, d] = send(*self.own(False, d), self.slot(0, -d))
 
@@ -194,7 +198,8 @@
                 for f in (0, -1, -3, -2):
                     self.waits[f, e].wait_recv()
 
-    in_cols = pl.ds(0, 512)
+    in_cols = pl.ds(0, 256)
+    query_cols = pl.ds(256, 128)
     out_cols = pl.ds(512, 128)
     phase("start")
     first = Gather(lambda zz, yy: w1.at[zz, yy, c], True)
@@ -204,33 +209,40 @@
     out_twin = Gather(
         lambda zz, yy: w2.at[x, zz, yy, o], False, stage.at[o, :, out_cols], w2.at[x, z, y, c]
     )
+    query = Gather(lambda zz, yy: wq.at[zz, yy, c], True)
+    query_twin = Gather(lambda zz, yy: wq.at[zz, yy, o], False, stage.at[o, :, query_cols], wq.at[z, y, c])
+    keys = Gather(lambda zz, yy: wkv.at[zz, yy, c], True)
+    later = (query, query_twin, keys, out_twin)
     first.begin()
     second.begin()
-    out_twin.begin()
+    first.across()
+    second.across()
+    for ring in later:
+        ring.begin()
+        ring.across()
     for load in loads[11:]:
         load.wait()
-    tok_in = [send(tokens, tokens, dev_x(d), tok.at[m4(x - d), half_rows]) for d in (1, 3, 2)]
     w2_own = [
         send(stage.at[c, :, out_cols], w2.at[x, z, y, c], dev_x(d), w2.at[m4(x - d), z, y, c]) for d in (1, 3, 2)
     ]
+    tok_in = [send(tokens, tokens, dev_x(d), tok.at[m4(x - d), half_rows]) for d in (2, 1, 3)]
     w_swap = send(stage.at[o, :, in_cols], w1.at[z, y, c], partner, w1.at[z, y, o])
     tok_swap = [send(tokens, tokens, partner, tok.at[x, other_rows])]
+    wq_swap = send(stage.at[o, :, query_cols], wq.at[z, y, c], partner, wq.at[z, y, o])
     w2_swap = send(stage.at[o, :, out_cols], w2.at[x, z, y, c], partner, w2.at[x, z, y, o])
     phase("near")
     for d in (1, 3, 2):
         first.forward(d)
         second.forward(d)
-    for d in (1, 3, 2):
-        out_twin.forward(d)
-    for arrived in w2_own:
-        arrived.wait_recv()
-    out_low.begin()
-    out_high.begin()
     phase("tokens")
-    for d, arrived in zip((1, 3, 2), tok_in):
+    for d, arrived in zip((1, 3, 2), tok_in[1:] + tok_in[:1]):
         arrived.wait_recv()
         src = m4(x - d)
         tok_swap.append(send(tok.at[src, half_rows], tok.at[src, half_rows], partner, tok.at[src, other_rows]))
+    phase("near2")
+    for ring in later:
+        for d in (1, 3, 2):
+            ring.forward(d)
     phase("tokswap")
     for arrived in tok_swap:
         arrived.wait_recv()
@@ -244,27 +256,29 @@
     for k in range(4):
         normed[k] = (tok[k].astype(F32) * inv * gain[:, 256 * k : 256 * k + 256]).astype(BF16)
 
+    phase("outbegin")
+    for arrived in w2_own:
+        arrived.wait_recv()
+    for ring in (out_low, out_high):
+        ring.begin()
+        ring.across()
     phase("wfinish")
     w_swap.wait_recv()
     first.finish()
     second.finish()
 
     phase("proj")
-    proj = mm(normed[0], w1[0].reshape(256, 512))
-    for k in range(1, 4):
-        proj = proj + mm(normed[k], w1[k].reshape(256, 512))
+    def project(w):
+        total = mm(normed[0], w(0))
+        for k in range(1, 4):
+            total = total + mm(normed[k], w(k))
+        return total
+
+    proj = project(lambda k: w1[k].reshape(256, 256))
     phase("gates0")
-    t0, t1, t2 = proj[:, 0:128], proj[:, 128:256], proj[:, 256:384]
-    kv[64:320, :] = proj[:, 384:512].astype(BF16)
-    halo = [
-        send(kv.at[pl.ds(256, 64)], kv.at[pl.ds(0, 64)], dev_b(1), kv.at[pl.ds(0, 64)]),
-        send(kv.at[pl.ds(64, 64)], kv.at[pl.ds(320, 64)], dev_b(-1), kv.at[pl.ds(320, 64)]),
-    ]
+    t1, t2 = proj[:, 0:128], proj[:, 128:256]
     lane = lax.broadcasted_iota(jnp.int32, (1, 128), 1)
     head = lane < 64
-    act = silu(t0.astype(BF16).astype(F32))
-    act = jnp.where(head, act, 0.0)
-    q = act * (lax.rsqrt(jnp.sum(act * act, axis=-1, keepdims=True) + EPS) * HEAD_DIM**-0.5)
     act = silu(t1.astype(BF16).astype(F32))
     act_k = jnp.where(head, act, 0.0)
     key_val = jnp.where(head, act * lax.rsqrt(jnp.sum(act_k * act_k, axis=-1, keepdims=True) + EPS), act)
@@ -298,25 +312,17 @@
     )
     turned = jnp.where(head, key_val, g_all).T
     key_t = turned[0:64]
-    q_left, key_left = left(q), left(key_val)
-
-    phase("rings")
-    w2_swap.wait_recv()
-    for d in (1, 3, 2):
-        out_low.forward(d)
-        out_high.forward(d)
-    out_twin.finish()
-    w2_in = [send(w2.at[x, :, :, o], w2.at[x, :, :, o], dev_x(d), w2.at[m4(x - d), :, :, o]) for d in (1, 3, 2)]
+    key_left = left(key_val)
 
     phase("delta1")
     lane2 = lax.broadcasted_iota(jnp.int32, (64, 128), 1)
     row2 = lax.broadcasted_iota(jnp.int32, (64, 128), 0)
     eye2 = jnp.where(lane2 == row2, 1.0, 0.0)
     chains = [(way, h) for way in range(2) for h in range(2)]
-    low, scores_d, sides, grown, key_end, end = {}, {}, {}, {}, {}, {}
+    low, decays, sides, grown, key_end, end = {}, {}, {}, {}, {}, {}
     for h in range(2):
         hs = slice(128 * h, 128 * h + 128)
-        pairs = mm(jnp.concatenate([q_left[hs], key_left[hs]], axis=0), right64(key_t[:, hs]))
+        pairs = mm(key_left[hs], right64(key_t[:, hs]))
         pairs = pairs[:, 0:128] + pairs[:, 128:256]
         for way in range(2):
             at = way, h
@@ -324,11 +330,10 @@
             g_col = g_all[hs, 66 + way : 67 + way]
             g_row = turned[66 + way : 67 + way, hs]
             g_end = g_col[127:128] if way == 0 else g_col[0:1]
-            decays = jnp.exp(jnp.where(masks[way], g_col - g_row, -jnp.inf))
-            low[at] = jnp.where(row == col, 0.0, beta * pairs[128:256] * decays)
-            scores_d[at] = pairs[0:128] * decays
+            decays[at] = jnp.exp(jnp.where(masks[way], g_col - g_row, -jnp.inf))
+            low[at] = jnp.where(row == col, 0.0, beta * pairs * decays[at])
             up = jnp.exp(g_col)
-            grown[at] = up * q[hs]
+            grown[at] = up
             sides[at] = key_val[hs] * jnp.where(head, beta * up, beta)
             key_end[at] = key_t[:, hs] * jnp.exp(g_end - g_row)
             end[at] = jnp.exp(g_end)
@@ -341,6 +346,13 @@
     d8 = {at: dot3(d4[at], d4[at]) for at in chains}
     inner = {at: inner[at] + dot3(inner[at], d4[at]) for at in chains}
     inner = {at: inner[at] + dot3(inner[at], d8[at]) for at in chains}
+    phase("rings")
+    keys.finish()
+    kv_swap = send(wkv.at[:, :, c], wkv.at[:, :, c], partner, wkv.at[:, :, o])
+    w2_swap.wait_recv()
+    out_twin.finish()
+    w2_in = [send(w2.at[x, :, :, o], w2.at[x, :, :, o], dev_x(d), w2.at[m4(x - d), :, :, o]) for d in (1, 3, 2)]
+
     phase("delta2")
     m1 = {at: dot3(inner[at], off[at]) for at in chains}
     wu = {at: dot3(inner[at], sides[at]) for at in chains}
@@ -349,6 +361,10 @@
     m4_ = {at: dot3(m2[at], m2[at]) for at in chains}
     wu = {at: wu[at] + dot3(m2[at], wu[at]) for at in chains}
     wu = {at: wu[at] + dot3(m4_[at], wu[at]) for at in chains}
+    phase("outfwd")
+    for d in (1, 3, 2):
+        out_low.forward(d)
+        out_high.forward(d)
     phase("final")
 
     def after(later, earlier):
@@ -360,6 +376,13 @@
         maps[at] = jnp.where(lane2 < 64, (end[at] - 1.0) * eye2 - final, final)
     for way in range(2):
         own_map[way] = after(maps[way, 1 - way], maps[way, way]).astype(LINK)
+    phase("kvproj")
+    kv_swap.wait_recv()
+    kv[64:320, :] = project(lambda k: wkv[k].reshape(256, 128)).astype(BF16)
+    halo = [
+        send(kv.at[pl.ds(256, 64)], kv.at[pl.ds(0, 64)], dev_b(1), kv.at[pl.ds(0, 64)]),
+        send(kv.at[pl.ds(64, 64)], kv.at[pl.ds(320, 64)], dev_b(-1), kv.at[pl.ds(320, 64)]),
+    ]
     phase("scan1send")
     scan = []
     steps = [(dz, dy) for dz in range(4) for dy in range(4) if (dz, dy) != (0, 0)]
@@ -369,12 +392,26 @@
         scan.append(
             send(own_map.at[goes], maps_in.at[z, y], dev(zz, yy, c, x), maps_in.at[m4(z - dz), m4(y - dy)])
         )
+    phase("qproj")
+    wq_swap.wait_recv()
+    query.finish()
+    query_twin.finish()
+    t0 = project(lambda k: wq[k].reshape(256, 128))
+    act = jnp.where(head, silu(t0.astype(BF16).astype(F32)), 0.0)
+    q = act * (lax.rsqrt(jnp.sum(act * act, axis=-1, keepdims=True) + EPS) * HEAD_DIM**-0.5)
+    q_left = left(q)
+
     phase("reads")
     reads = {}
+    pairs = []
+    for h in range(2):
+        hs = slice(128 * h, 128 * h + 128)
+        pair = mm(q_left[hs], right64(key_t[:, hs]))
+        pairs.append(pair[:, 0:128] + pair[:, 128:256])
     for way, h in chains:
         at = way, h
-        read = dot3(scores_d[at], wu[at])
-        reads[at] = jnp.where(head, grown[at] - read, read)
+        read = dot3(pairs[h] * decays[at], wu[at])
+        reads[at] = jnp.where(head, grown[at] * q[128 * h : 128 * h + 128] - read, read)
         if h != way:
             reads[at] = reads[at] + dot64(reads[at], maps[way, way])
     reads = [jnp.concatenate([reads[way, 0], reads[way, 1]], axis=0) for way in range(2)]
@@ -435,7 +472,7 @@
         hsend[k, 0:32] = heads[32 * k : 32 * k + 32]
         hsend[k, 32:64] = heads[128 + 32 * k : 160 + 32 * k]
     phase("headsend")
-    head_in = [send(hsend.at[m4(x + d)], hall.at[x], dev_x(d), hall.at[m4(x - d)]) for d in (1, 3, 2)]
+    head_in = [send(hsend.at[m4(x + d)], hall.at[x], dev_x(d), hall.at[m4(x - d)]) for d in (2, 1, 3)]
     hall[x] = hsend[x]
     phase("w2finish")
     out_low.finish()
@@ -447,15 +484,20 @@
         arrived.wait_recv()
     phase("outmm")
     gathered = jnp.concatenate([hall[k] for k in range(4)], axis=1)
+    last = []
     for k in range(4):
         rows = jnp.concatenate([w2[kx, k].reshape(256, 128) for kx in range(4)], axis=1)
         part = mm(gathered, rows, NT)
-        pbuf[0, :, 256 * k : 256 * k + 256] = part[0:32]
-        pbuf[1, :, 256 * k : 256 * k + 256] = part[32:64]
+        pbuf[k, 0] = part[0:32]
+        pbuf[k, 1] = part[32:64]
+        if k % 2:
+            pair = pl.ds(k - 1, 2)
+            last.append(send(pbuf.at[pair, o], prec.at[pair], partner, prec.at[pair]))
     phase("last")
-    last = send(pbuf.at[o], prec, partner, prec)
-    last.wait_recv()
-    out[...] = pbuf[c] + prec[...]
+    for k in range(4):
+        if k % 2 == 0:
+            last[k // 2].wait_recv()
+        out[:, 256 * k : 256 * k + 256] = pbuf[k, c] + prec[k]
     phase("drain")
     for copy in sent:
         copy.wait_send()
@@ -498,15 +540,17 @@
             pltpu.VMEM((4, 256, 256), BF16),
             pltpu.VMEM((4, 256, 256), BF16),
             pltpu.VMEM((2, 32, 640), BF16),
-            pltpu.VMEM((4, 4, 2, 32, 512), BF16),
+            pltpu.VMEM((4, 4, 2, 32, 256), BF16),
+            pltpu.VMEM((4, 4, 2, 32, 128), BF16),
+            pltpu.VMEM((4, 4, 2, 32, 128), BF16),
             pltpu.VMEM((4, 4, 4, 2, 32, 128), BF16),
             pltpu.VMEM((384, 128), BF16),
             pltpu.VMEM((2, 64, 128), LINK),
             pltpu.VMEM((4, 4, 64, 128), LINK),
             pltpu.VMEM((4, 64, 128), BF16),
             pltpu.VMEM((4, 64, 128), BF16),
-            pltpu.VMEM((2, 32, 1024), F32),
-            pltpu.VMEM((32, 1024), F32),
+            pltpu.VMEM((4, 2, 32, 256), F32),
+            pltpu.VMEM((4, 32, 256), F32),
             pltpu.SemaphoreType.DMA((COPIES,)),
             pltpu.SemaphoreType.DMA((COPIES,)),
             pltpu.SemaphoreType.DMA((18,)),

time: 39.7 us -> 38.3 us (0.965)
  Pallas kernels: 38.9 us -> 37.5 us
    pallas_call x1, Pallas kernels: 38.9 us -> 37.5 us  [per_device(): pl.pallas_call(layer_kernel, out_shape=jax.ShapeDtypeStruct((32, 1024), F...]
where the time goes in v7:
time: 38.3 us; the launch traced here: 38.1 us
  Pallas kernels  37.5 us (98%)
  other arithmetic  0.64 us (2%)
    pallas_call x1, Pallas kernels, per_device(): pl.pallas_call(layer_kernel, out_shape=jax.ShapeDtypeStruct((32, 1024), F...  37.5 us

profile of v7, /device:TPU:1, one launch (start us, length us, event | category | flops | bytes accessed | tf_op | source)
XLA Modules:
  0.0 38.1 jit_solution(1636002160279984912)
XLA Ops:
  0.0 37.5 %shard_map.163 = f32[32,1024]{1,0:T(8,128)S(1)} custom-call(bf16[128,256]{1,0:T(8,128)(2,1)} %tokens_in.1, f32[1,1024]{1,0:T(1,128)} %bitcast.8, bf16[32,128]{1,0:T(8,128)(2,1)} %aq_in.1, bf16[32,64]{1,0:T(8,128)(2,1)} %ak_in.1, bf16[32,64]{1,0:T(8,128)(2,1)} %av_in.1, bf16[32,128]{1,0:T(8,128)(2,1)} %dq_in.1, bf16[32,128]{1,0:T(8,128)(2,1)} %dk_in.1, ...), custom_call_target="tpu_custom_call" | custom-call | tf_op jit(solution)/shard_map/pallas_call | solution.py:518
  37.5 0.6 %convert_element_type.3 = bf16[32,1024]{1,0:T(8,128)(2,1)} convert(f32[32,1024]{1,0:T(8,128)S(1)} %shard_map.163) | non-fusion elementwise | flops 32768 | bytes 196608 | tf_op jit(solution)/shard_map/convert_element_type | solution.py:560

commit v8 on v7

--- a/solution.py
+++ b/solution.py
@@ -361,10 +361,6 @@
     m4_ = {at: dot3(m2[at], m2[at]) for at in chains}
     wu = {at: wu[at] + dot3(m2[at], wu[at]) for at in chains}
     wu = {at: wu[at] + dot3(m4_[at], wu[at]) for at in chains}
-    phase("outfwd")
-    for d in (1, 3, 2):
-        out_low.forward(d)
-        out_high.forward(d)
     phase("final")
 
     def after(later, earlier):
@@ -441,6 +437,10 @@
     phase("scanwait")
     for arrived in scan:
         arrived.wait_recv()
+    phase("outfwd")
+    for d in (1, 3, 2):
+        out_low.forward(d)
+        out_high.forward(d)
     phase("states")
     states = []
     for way in range(2):

time: 38.3 us -> 37 us (0.966)
  Pallas kernels: 37.5 us -> 36.2 us
    pallas_call x1, Pallas kernels: 37.5 us -> 36.2 us  [per_device(): pl.pallas_call(layer_kernel, out_shape=jax.ShapeDtypeStruct((32, 1024), F...]
where the time goes in v8:
time: 37 us; the launch traced here: 36.8 us
  Pallas kernels  36.2 us (98%)
  other arithmetic  0.64 us (2%)
    pallas_call x1, Pallas kernels, per_device(): pl.pallas_call(layer_kernel, out_shape=jax.ShapeDtypeStruct((32, 1024), F...  36.2 us

profile of v8, /device:TPU:1, one launch (start us, length us, event | category | flops | bytes accessed | tf_op | source)
XLA Modules:
  0.0 36.8 jit_solution(683978832703184216)
XLA Ops:
  0.0 36.2 %shard_map.163 = f32[32,1024]{1,0:T(8,128)S(1)} custom-call(bf16[128,256]{1,0:T(8,128)(2,1)} %tokens_in.1, f32[1,1024]{1,0:T(1,128)} %bitcast.8, bf16[32,128]{1,0:T(8,128)(2,1)} %aq_in.1, bf16[32,64]{1,0:T(8,128)(2,1)} %ak_in.1, bf16[32,64]{1,0:T(8,128)(2,1)} %av_in.1, bf16[32,128]{1,0:T(8,128)(2,1)} %dq_in.1, bf16[32,128]{1,0:T(8,128)(2,1)} %dk_in.1, ...), custom_call_target="tpu_custom_call" | custom-call | tf_op jit(solution)/shard_map/pallas_call | solution.py:518
  36.2 0.6 %convert_element_type.3 = bf16[32,1024]{1,0:T(8,128)(2,1)} convert(f32[32,1024]{1,0:T(8,128)S(1)} %shard_map.163) | non-fusion elementwise | flops 32768 | bytes 196608 | tf_op jit(solution)/shard_map/convert_element_type | solution.py:560

commit v9 on v8

--- a/solution.py
+++ b/solution.py
@@ -204,7 +204,7 @@
     phase("start")
     first = Gather(lambda zz, yy: w1.at[zz, yy, c], True)
     second = Gather(lambda zz, yy: w1.at[zz, yy, o], False, stage.at[o, :, in_cols], w1.at[z, y, c])
-    out_low = Gather(lambda zz, yy: w2.at[:, zz, yy, c, pl.ds(0, 16)], True)
+    out_low = Gather(lambda zz, yy: w2.at[x, zz, yy, c, pl.ds(0, 16)], True)
     out_high = Gather(lambda zz, yy: w2.at[:, zz, yy, c, pl.ds(16, 16)], False)
     out_twin = Gather(
         lambda zz, yy: w2.at[x, zz, yy, o], False, stage.at[o, :, out_cols], w2.at[x, z, y, c]
@@ -212,7 +212,7 @@
     query = Gather(lambda zz, yy: wq.at[zz, yy, c], True)
     query_twin = Gather(lambda zz, yy: wq.at[zz, yy, o], False, stage.at[o, :, query_cols], wq.at[z, y, c])
     keys = Gather(lambda zz, yy: wkv.at[zz, yy, c], True)
-    later = (query, query_twin, keys, out_twin)
+    later = (query, query_twin, keys, out_twin, out_low)
     first.begin()
     second.begin()
     first.across()
@@ -222,8 +222,12 @@
         ring.across()
     for load in loads[11:]:
         load.wait()
+    upper = pl.ds(16, 16)
     w2_own = [
-        send(stage.at[c, :, out_cols], w2.at[x, z, y, c], dev_x(d), w2.at[m4(x - d), z, y, c]) for d in (1, 3, 2)
+        send(
+            stage.at[c, upper, out_cols], w2.at[x, z, y, c, upper], dev_x(d), w2.at[m4(x - d), z, y, c, upper]
+        )
+        for d in (1, 3, 2)
     ]
     tok_in = [send(tokens, tokens, dev_x(d), tok.at[m4(x - d), half_rows]) for d in (2, 1, 3)]
     w_swap = send(stage.at[o, :, in_cols], w1.at[z, y, c], partner, w1.at[z, y, o])
@@ -259,9 +263,8 @@
     phase("outbegin")
     for arrived in w2_own:
         arrived.wait_recv()
-    for ring in (out_low, out_high):
-        ring.begin()
-        ring.across()
+    out_high.begin()
+    out_high.across()
     phase("wfinish")
     w_swap.wait_recv()
     first.finish()
@@ -351,7 +354,15 @@
     kv_swap = send(wkv.at[:, :, c], wkv.at[:, :, c], partner, wkv.at[:, :, o])
     w2_swap.wait_recv()
     out_twin.finish()
-    w2_in = [send(w2.at[x, :, :, o], w2.at[x, :, :, o], dev_x(d), w2.at[m4(x - d), :, :, o]) for d in (1, 3, 2)]
+    out_low.finish()
+    w2_in = []
+    for d in (1, 3, 2):
+        src = m4(x - d)
+        lower = pl.ds(0, 16)
+        w2_in.append(send(w2.at[x, :, :, o], w2.at[x, :, :, o], dev_x(d), w2.at[src, :, :, o]))
+        w2_in.append(
+            send(w2.at[x, :, :, c, lower], w2.at[x, :, :, c, lower], dev_x(d), w2.at[src, :, :, c, lower])
+        )
 
     phase("delta2")
     m1 = {at: dot3(inner[at], off[at]) for at in chains}
@@ -372,6 +383,20 @@
         maps[at] = jnp.where(lane2 < 64, (end[at] - 1.0) * eye2 - final, final)
     for way in range(2):
         own_map[way] = after(maps[way, 1 - way], maps[way, way]).astype(LINK)
+    phase("scan1send")
+    scan = []
+
+    def send_map(dz, dy):
+        zz, yy = m4(z + dz), m4(y + dy)
+        goes = jnp.where(zz * 4 + yy > b, 0, 1)
+        scan.append(
+            send(own_map.at[goes], maps_in.at[z, y], dev(zz, yy, c, x), maps_in.at[m4(z - dz), m4(y - dy)])
+        )
+
+    steps = [(dz, dy) for dz in range(4) for dy in range(4) if (dz, dy) != (0, 0)]
+    steps.sort(key=lambda step: -(min(step[0], 4 - step[0]) + min(step[1], 4 - step[1])))
+    for dz, dy in steps[:5]:
+        send_map(dz, dy)
     phase("kvproj")
     kv_swap.wait_recv()
     kv[64:320, :] = project(lambda k: wkv[k].reshape(256, 128)).astype(BF16)
@@ -379,15 +404,9 @@
         send(kv.at[pl.ds(256, 64)], kv.at[pl.ds(0, 64)], dev_b(1), kv.at[pl.ds(0, 64)]),
         send(kv.at[pl.ds(64, 64)], kv.at[pl.ds(320, 64)], dev_b(-1), kv.at[pl.ds(320, 64)]),
     ]
-    phase("scan1send")
-    scan = []
-    steps = [(dz, dy) for dz in range(4) for dy in range(4) if (dz, dy) != (0, 0)]
-    for dz, dy in sorted(steps, key=lambda step: -(min(step[0], 4 - step[0]) + min(step[1], 4 - step[1]))):
-        zz, yy = m4(z + dz), m4(y + dy)
-        goes = jnp.where(zz * 4 + yy > b, 0, 1)
-        scan.append(
-            send(own_map.at[goes], maps_in.at[z, y], dev(zz, yy, c, x), maps_in.at[m4(z - dz), m4(y - dy)])
-        )
+    phase("scan1send2")
+    for dz, dy in steps[5:]:
+        send_map(dz, dy)
     phase("qproj")
     wq_swap.wait_recv()
     query.finish()
@@ -439,7 +458,6 @@
         arrived.wait_recv()
     phase("outfwd")
     for d in (1, 3, 2):
-        out_low.forward(d)
         out_high.forward(d)
     phase("states")
     states = []
@@ -475,21 +493,22 @@
     head_in = [send(hsend.at[m4(x + d)], hall.at[x], dev_x(d), hall.at[m4(x - d)]) for d in (2, 1, 3)]
     hall[x] = hsend[x]
     phase("w2finish")
-    out_low.finish()
     out_high.finish()
     for arrived in w2_in:
         arrived.wait_recv()
     phase("headwait")
-    for arrived in head_in:
-        arrived.wait_recv()
+    def head_part(k):
+        return mm(hall[k], w2[k].reshape(1024, 128), NT)
+
+    part = head_part(x)
+    for d, arrived in zip((1, 3, 2), head_in[1:] + head_in[:1]):
+        arrived.wait_recv()
+        part = part + head_part(m4(x - d))
     phase("outmm")
-    gathered = jnp.concatenate([hall[k] for k in range(4)], axis=1)
     last = []
     for k in range(4):
-        rows = jnp.concatenate([w2[kx, k].reshape(256, 128) for kx in range(4)], axis=1)
-        part = mm(gathered, rows, NT)
-        pbuf[k, 0] = part[0:32]
-        pbuf[k, 1] = part[32:64]
+        pbuf[k, 0] = part[0:32, 256 * k : 256 * k + 256]
+        pbuf[k, 1] = part[32:64, 256 * k : 256 * k + 256]
         if k % 2:
             pair = pl.ds(k - 1, 2)
             last.append(send(pbuf.at[pair, o], prec.at[pair], partner, prec.at[pair]))

time: 37 us -> 37 us (level)
  no operation moved by 1% of the time
where the time goes in v9:
time: 37 us; the launch traced here: 36.9 us
  Pallas kernels  36.2 us (98%)
  other arithmetic  0.64 us (2%)
    pallas_call x1, Pallas kernels, per_device(): pl.pallas_call(layer_kernel, out_shape=jax.ShapeDtypeStruct((32, 1024), F...  36.2 us

profile of v9, /device:TPU:1, one launch (start us, length us, event | category | flops | bytes accessed | tf_op | source)
XLA Modules:
  0.0 36.9 jit_solution(8652599329552108780)
XLA Ops:
  0.0 36.2 %shard_map.163 = f32[32,1024]{1,0:T(8,128)S(1)} custom-call(bf16[128,256]{1,0:T(8,128)(2,1)} %tokens_in.1, f32[1,1024]{1,0:T(1,128)} %bitcast.8, bf16[32,128]{1,0:T(8,128)(2,1)} %aq_in.1, bf16[32,64]{1,0:T(8,128)(2,1)} %ak_in.1, bf16[32,64]{1,0:T(8,128)(2,1)} %av_in.1, bf16[32,128]{1,0:T(8,128)(2,1)} %dq_in.1, bf16[32,128]{1,0:T(8,128)(2,1)} %dk_in.1, ...), custom_call_target="tpu_custom_call" | custom-call | tf_op jit(solution)/shard_map/pallas_call | solution.py:537
  36.3 0.6 %convert_element_type.3 = bf16[32,1024]{1,0:T(8,128)(2,1)} convert(f32[32,1024]{1,0:T(8,128)S(1)} %shard_map.163) | non-fusion elementwise | flops 32768 | bytes 196608 | tf_op jit(solution)/shard_map/convert_element_type | solution.py:579
